TPU v7x, 32 devices: a whole 2x2x4 slice. The times are simulated.
32 devices in a mesh: sp: 8 (over z, x), tp: 4 (over y, core).
Axes of the slice: x: 2, y: 2, z: 4, core: 2. Of those that a mesh axis runs over, the one named last changes fastest.
Arguments:
- lane_source_signal: bfloat16 [1024, 1024], P('tp', 'sp'), may hold values from -6 to 6
- spectral_damping_part: float32 [64, 64], P('tp'), may hold values from -3 to -0.0002
- spectral_angular_part: float32 [64, 64], P('tp'), may hold values from 0.31 to 201.0624
- interval_exponent: float32 [64], P('tp'), may hold values from -3.9 to -1.6
- entry_matrix_inphase: float32 [64, 64, 16], P('tp'), may hold values from -1 to 1
- entry_matrix_quadrature: float32 [64, 64, 16], P('tp'), may hold values from -1 to 1
- emission_inphase: float32 [64, 16, 64], P('tp'), may hold values from -0.75 to 0.75
- emission_quadrature: float32 [64, 16, 64], P('tp'), may hold values from -0.75 to 0.75
- lane_bypass_factor: float32 [1024], P('tp'), may hold values from -5 to 5
- spike_shrink_offset: float32 [64, 1024], P('tp', 'sp'), may hold values from -1.4 to 0
- lane_exit_matrix: bfloat16 [1024, 4096], P('tp'), may hold values from -0.1875 to 0.1875
- skipline_stream: bfloat16 [1024, 4096], P('sp'), may hold values from -6 to 6
- specialist_scaling_vector: float32 [4096], replicated, may hold values from 0.1 to 1.9
- selected_specialists: int32 [1024, 2], P('sp'), may hold values from 0 to 7, all different within a row; in each aligned block of 128 rows (0 to 127, 128 to 255, ...) at most 64 rows name the same one
- dispatcher_scores: float32 [1024, 2], P('sp'), may hold values from 0.1 to 1
- specialist_valve_matrix: bfloat16 [8, 4096, 2048], P('sp', None, 'tp'), may hold values from -0.09375 to 0.09375
- specialist_widen_matrix: bfloat16 [8, 4096, 2048], P('sp', None, 'tp'), may hold values from -0.09375 to 0.09375
- specialist_shrink_matrix: bfloat16 [8, 2048, 4096], P('sp', 'tp'), may hold values from -0.1875 to 0.1875
Outputs:
- updated: bfloat16 [1024, 4096], P('sp', 'tp')
Inputs may be any that keep to these rules, and one draw needn't show every extreme that they name: `selected_specialists`: each row names 2 different experts. Among the rows of each aligned block of 128 positions no expert is named more than 64 times, and in every block some expert is named exactly 64 times.
All inputs are finite; a program needn't handle non-finite values.
Results may differ from a plain program's by a relative error of at most 0.019.
Values may be sent and summed in bfloat16 or wider, within the bound.
A program may use at most 64 MiB of HBM per device.

v0:
```python
import jax
import jax.numpy as jnp
from jax import lax
from jax.experimental import pallas as pl
from jax.experimental.pallas import tpu as pltpu
from jax.sharding import PartitionSpec as P

EPS = 1e-06
PRECISE_MODE = lax.Precision.HIGHEST


MESH = pl.DeviceIdType.MESH
VM = pl.BlockSpec(memory_space=pltpu.VMEM)
DMA = pltpu.SemaphoreType.DMA
VMEM_ROOM = 48 * 1024 * 1024


def greet(peers):
    barrier = pltpu.get_barrier_semaphore()
    for peer in peers:
        pl.semaphore_signal(barrier, inc=1, device_id=peer, device_id_type=MESH)
    pl.semaphore_wait(barrier, len(peers))


def remote(src, dst, send, recv, where):
    return pltpu.make_async_remote_copy(
        src_ref=src, dst_ref=dst, send_sem=send, recv_sem=recv, device_id=where, device_id_type=MESH
    )


def places():
    n_sp, n_tp = lax.axis_size("sp"), lax.axis_size("tp")
    return n_sp, n_tp, lax.axis_index("sp"), lax.axis_index("tp")


def carry_kernel(mine, out, pieces, send, recv):
    n_sp, n_tp, me, lane = places()
    greet([(lax.rem(me + i, n_sp), lane) for i in range(1, n_sp)])
    copies = []
    for i in range(1, n_sp):
        copy = remote(
            mine, pieces.at[i - 1], send.at[i - 1], recv.at[i - 1], (lax.rem(me + i, n_sp), lane)
        )
        copy.start()
        copies.append(copy)
    for copy in copies:
        copy.wait_recv()
    run_re = jnp.zeros(mine.shape[1:], jnp.float32)
    run_im = run_re
    for i in range(n_sp - 1, 0, -1):
        mul_re, mul_im, add_re, add_im = (pieces[i - 1, plane] for plane in range(4))
        new_re = mul_re * run_re - mul_im * run_im + add_re
        new_im = mul_re * run_im + mul_im * run_re + add_im
        run_re = jnp.where(me >= i, new_re, run_re)
        run_im = jnp.where(me >= i, new_im, run_im)
    out[0] = run_re
    out[1] = run_im
    for copy in copies:
        copy.wait_send()


def carry_call(summary):
    n_sp = lax.axis_size("sp")
    return pl.pallas_call(
        carry_kernel,
        out_shape=jax.ShapeDtypeStruct((2,) + summary.shape[1:], jnp.float32),
        in_specs=[VM],
        out_specs=VM,
        scratch_shapes=[
            pltpu.VMEM((n_sp - 1,) + summary.shape, jnp.float32),
            DMA((n_sp - 1,)),
            DMA((n_sp - 1,)),
        ],
        compiler_params=pltpu.CompilerParams(collective_id=0, has_side_effects=True),
        name="carry",
    )(summary)


def tp_peers(n_tp, me, lane):
    return [(me, lax.rem(lane + i, n_tp)) for i in range(1, n_tp)]


def sp_peers(n_sp, me, lane):
    return [(lax.rem(me + i, n_sp), lane) for i in range(1, n_sp)]


def dispatch_kernel(
    rows, w, skip, gain, hot,
    stream_out, xs,
    psend, precv, ysend, yrecv, ssend, srecv, dsend,
    ps, pr, ys, yr, ss, sr, ds, dr, fs, fr, qs, qr,
):
    f32, bf16 = jnp.float32, jnp.bfloat16
    n_sp, n_tp, me, lane = places()
    n_y = n_tp // 2
    y, core = lane // 2, lax.rem(lane, 2)
    partner = (me, y * 2 + 1 - core)
    d_local = stream_out.shape[1]
    cap = hot.shape[0] // n_sp
    greet(tp_peers(n_tp, me, lane) + sp_peers(n_sp, me, lane))

    def cols(block):
        return pl.ds(pl.multiple_of(block * d_local, 128), d_local)

    def rows_of(source):
        return pl.ds(pl.multiple_of(source * cap, 16), cap)

    def part(block):
        return jnp.dot(rows[...], w[:, cols(block)], preferred_element_type=f32)

    def y_at(i):
        return lax.rem(y + i, n_y)

    waits = []

    def go(copy):
        copy.start()
        waits.append(copy)
        return copy

    pair = []
    for i in range(n_y - 1, -1, -1):
        psend[i] = part(y_at(i) * 2 + 1 - core).astype(bf16)
        pair.append(go(remote(psend.at[i], precv.at[i], ps.at[i], pr.at[i], partner)))
    pair = pair[::-1]
    across = []
    for i in range(n_y - 1, 0, -1):
        own = part(y_at(i) * 2 + core)
        pair[i].wait_recv()
        ysend[i - 1] = (own + precv[i].astype(f32)).astype(bf16)
        across.append(
            go(
                remote(
                    ysend.at[i - 1], yrecv.at[i - 1], ys.at[i - 1], yr.at[i - 1],
                    (me, y_at(i) * 2 + core),
                )
            )
        )
    total = part(lane)
    pair[0].wait_recv()
    total = total + precv[0].astype(f32)
    for i, copy in enumerate(across[::-1]):
        copy.wait_recv()
        total = total + yrecv[i].astype(f32)
    projected = total.astype(bf16).astype(f32)
    stream = (skip[:, cols(lane)].astype(f32) + projected).astype(bf16)
    stream_out[...] = stream
    stream_f = stream.astype(f32)
    tok = stream_f.shape[0]
    square = jnp.sum(stream_f * stream_f, axis=1, keepdims=True)
    as_rows = jnp.broadcast_to(square, (tok, 128)).T[0:8, :]
    ssend[...] = as_rows
    sums = []
    for i in range(1, n_tp):
        sums.append(
            go(
                remote(
                    ssend, srecv.at[i - 1], ss.at[i - 1], sr.at[i - 1], (me, lax.rem(lane + i, n_tp))
                )
            )
        )
    for i, copy in enumerate(sums):
        copy.wait_recv()
        as_rows = as_rows + srecv[i]
    width = n_tp * d_local
    inv = lax.rsqrt(as_rows / width + EPS)
    inv_rms = jnp.broadcast_to(inv[0:1, :], (128, tok)).T[:, 0:1]
    normed = (stream_f * inv_rms * gain[0:1, cols(lane)]).astype(bf16)

    out_cols = cols(lane)
    arrivals = []
    for i in range(1, n_sp):
        to = lax.rem(me + i, n_sp)
        dsend[i - 1] = jnp.dot(hot[rows_of(to), :], normed, preferred_element_type=f32).astype(bf16)
        arrivals.append(
            go(
                remote(
                    dsend.at[i - 1], xs.at[rows_of(me), out_cols], ds.at[i - 1], dr.at[i - 1],
                    (to, lane),
                )
            )
        )
    xs[rows_of(me), out_cols] = jnp.dot(
        hot[rows_of(me), :], normed, preferred_element_type=f32
    ).astype(bf16)

    def spread(n, source):
        there = xs.at[rows_of(source), out_cols]
        for i in range(1, n_y):
            k = (i - 1) * n_sp + n
            go(remote(there, there, fs.at[k], fr.at[k], (me, y_at(i) * 2 + core)))
        go(remote(there, there, qs.at[n], qr.at[n], partner))

    def source_at(n):
        return lax.rem(me + n_sp - n, n_sp)

    def landed(source, block, recv, send):
        here = xs.at[rows_of(source), cols(block)]
        remote(here, here, send, recv, partner).wait_recv()

    spread(0, me)
    for n in range(1, n_sp):
        landed(source_at(n), lane, dr.at[n - 1], ds.at[n - 1])
        spread(n, source_at(n))
    for n in range(n_sp):
        for i in range(1, n_y):
            k = (i - 1) * n_sp + n
            from_block = lax.rem(y + n_y - i, n_y) * 2 + core
            landed(source_at(n), from_block, fr.at[k], fs.at[k])
            here = xs.at[rows_of(source_at(n)), cols(from_block)]
            q = i * n_sp + n
            go(remote(here, here, qs.at[q], qr.at[q], partner))
    for n in range(n_sp):
        for i in range(n_y):
            from_block = lax.rem(y + n_y - i, n_y) * 2 + 1 - core
            q = i * n_sp + n
            landed(source_at(n), from_block, qr.at[q], qs.at[q])
    for copy in waits:
        copy.wait_send()


def dispatch_call(rows, w, skip, gain, hot):
    n_sp, n_tp = lax.axis_size("sp"), lax.axis_size("tp")
    n_y = n_tp // 2
    bf16, f32 = jnp.bfloat16, jnp.float32
    tok, width = skip.shape
    d_local = width // n_tp
    slots = hot.shape[0]
    cap = slots // n_sp
    more = max(n_y - 1, 1)
    return pl.pallas_call(
        dispatch_kernel,
        out_shape=(
            jax.ShapeDtypeStruct((tok, d_local), bf16),
            jax.ShapeDtypeStruct((slots, width), bf16),
        ),
        in_specs=[VM] * 5,
        out_specs=(VM, VM),
        scratch_shapes=[
            pltpu.VMEM((n_y, tok, d_local), bf16),
            pltpu.VMEM((n_y, tok, d_local), bf16),
            pltpu.VMEM((more, tok, d_local), bf16),
            pltpu.VMEM((more, tok, d_local), bf16),
            pltpu.VMEM((8, tok), f32),
            pltpu.VMEM((n_tp - 1, 8, tok), f32),
            pltpu.VMEM((n_sp - 1, cap, d_local), bf16),
            DMA((n_y,)),
            DMA((n_y,)),
            DMA((more,)),
            DMA((more,)),
            DMA((n_tp - 1,)),
            DMA((n_tp - 1,)),
            DMA((n_sp - 1,)),
            DMA((n_sp - 1,)),
            DMA((more * n_sp,)),
            DMA((more * n_sp,)),
            DMA((n_y * n_sp,)),
            DMA((n_y * n_sp,)),
        ],
        compiler_params=pltpu.CompilerParams(
            collective_id=1, has_side_effects=True, vmem_limit_bytes=VMEM_ROOM // 2
        ),
        name="dispatch",
    )(rows, w, skip, gain, hot)


def return_kernel(
    hidden, w, share, pick,
    out,
    psend, own, precv, ysend, yrecv, rsend, ret,
    ps, pr, ys, yr, rs, rr,
):
    f32, bf16 = jnp.float32, jnp.bfloat16
    n_sp, n_tp, me, lane = places()
    n_y = n_tp // 2
    y, core = lane // 2, lax.rem(lane, 2)
    partner = (me, y * 2 + 1 - core)
    d_local = out.shape[1]
    cap = hidden.shape[0] // n_sp
    greet(
        [partner]
        + [(me, lax.rem(y + i, n_y) * 2 + core) for i in range(1, n_y)]
        + sp_peers(n_sp, me, lane)
    )

    def cols(block):
        return pl.ds(pl.multiple_of(block * d_local, 128), d_local)

    def rows_of(source):
        return pl.ds(pl.multiple_of(source * cap, 16), cap)

    def y_at(i):
        return lax.rem(y + i, n_y)

    def to_at(n):
        return lax.rem(me + n + 1, n_sp)

    waits = []

    def go(copy):
        copy.start()
        waits.append(copy)
        return copy

    pair, across, back = {}, {}, []
    def part(n, block):
        return jnp.dot(hidden[rows_of(to_at(n)), :], w[:, cols(block)], preferred_element_type=f32)

    order = list(range(1, n_y)) + [0]
    for n in range(n_sp + 1):
        if n < n_sp:
            for i in order:
                k = n * n_y + i
                psend[k] = part(n, y_at(i) * 2 + 1 - core).astype(bf16)
                pair[n, i] = go(remote(psend.at[k], precv.at[k], ps.at[k], pr.at[k], partner))
            for i in order:
                own[n * n_y + i] = part(n, y_at(i) * 2 + core)
        if n > 0:
            for i in range(1, n_y):
                pair[n - 1, i].wait_recv()
                j = (n - 1) * n_y + i
                k = (n - 1) * (n_y - 1) + i - 1
                ysend[k] = (own[j] + precv[j].astype(f32)).astype(bf16)
                across[n - 1, i] = go(
                    remote(
                        ysend.at[k], yrecv.at[k], ys.at[k], yr.at[k], (me, y_at(i) * 2 + core)
                    )
                )
    for n in range(n_sp):
        total = own[n * n_y]
        pair[n, 0].wait_recv()
        total = total + precv[n * n_y].astype(f32)
        for i in range(1, n_y):
            across[n, i].wait_recv()
            total = total + yrecv[n * (n_y - 1) + i - 1].astype(f32)
        if n < n_sp - 1:
            rsend[n] = total.astype(bf16)
            back.append(
                go(remote(rsend.at[n], ret.at[rows_of(me), :], rs.at[n], rr.at[n], (to_at(n), lane)))
            )
        else:
            ret[rows_of(me), :] = total.astype(bf16)
    for n in range(n_sp - 1):
        here = ret.at[rows_of(lax.rem(me + n_sp - n - 1, n_sp)), :]
        remote(here, here, rs.at[n], rr.at[n], partner).wait_recv()
    rows_in = ret[...]
    moe = None
    for k in range(pick.shape[0]):
        chosen = jnp.dot(pick[k], rows_in, preferred_element_type=f32) * share[:, k : k + 1]
        moe = chosen if moe is None else moe + chosen
    out[...] = moe
    for copy in waits:
        copy.wait_send()


def return_call(hidden, w, share, pick):
    n_sp, n_tp = lax.axis_size("sp"), lax.axis_size("tp")
    n_y = n_tp // 2
    bf16, f32 = jnp.bfloat16, jnp.float32
    tok, d_local = share.shape[0], w.shape[1] // n_tp
    slots = hidden.shape[0]
    cap = slots // n_sp
    more = max((n_y - 1) * n_sp, 1)
    return pl.pallas_call(
        return_kernel,
        out_shape=jax.ShapeDtypeStruct((tok, d_local), f32),
        in_specs=[VM] * 4,
        out_specs=VM,
        scratch_shapes=[
            pltpu.VMEM((n_y * n_sp, cap, d_local), bf16),
            pltpu.VMEM((n_y * n_sp, cap, d_local), f32),
            pltpu.VMEM((n_y * n_sp, cap, d_local), bf16),
            pltpu.VMEM((more, cap, d_local), bf16),
            pltpu.VMEM((more, cap, d_local), bf16),
            pltpu.VMEM((n_sp - 1, cap, d_local), bf16),
            pltpu.VMEM((slots, d_local), bf16),
            DMA((n_y * n_sp,)),
            DMA((n_y * n_sp,)),
            DMA((more,)),
            DMA((more,)),
            DMA((n_sp - 1,)),
            DMA((n_sp - 1,)),
        ],
        compiler_params=pltpu.CompilerParams(
            collective_id=2, has_side_effects=True, vmem_limit_bytes=VMEM_ROOM
        ),
        name="combine",
    )(hidden, w, share, pick)


def affine_pair(earlier, latter):
    mul_re = earlier[0] * latter[0] - earlier[1] * latter[1]
    mul_im = earlier[0] * latter[1] + earlier[1] * latter[0]
    add_re = latter[0] * earlier[2] - latter[1] * earlier[3] + latter[2]
    add_im = latter[0] * earlier[3] + latter[1] * earlier[2] + latter[3]
    return (mul_re, mul_im, add_re, add_im)


def local_prefix(elements):
    length = elements[0].shape[2]
    fills = (1.0, 0.0, 0.0, 0.0)
    offset = 1
    while offset < length:
        earlier = tuple(
            (
                jnp.pad(
                    item[:, :, : length - offset],
                    ((0, 0), (0, 0), (offset, 0)),
                    constant_values=fill,
                )
                for item, fill in zip(elements, fills)
            )
        )
        elements = affine_pair(earlier, elements)
        offset = offset * 2
    return elements


def per_device(
    lane_source_signal,
    spectral_damping_part,
    spectral_angular_part,
    interval_exponent,
    entry_matrix_inphase,
    entry_matrix_quadrature,
    emission_inphase,
    emission_quadrature,
    lane_bypass_factor,
    spike_shrink_offset,
    lane_exit_matrix,
    skipline_stream,
    specialist_scaling_vector,
    selected_specialists,
    dispatcher_scores,
    specialist_valve_matrix,
    specialist_widen_matrix,
    specialist_shrink_matrix,
):
    f32 = jnp.float32
    bf16 = jnp.bfloat16
    groups_here = spectral_damping_part.shape[0]
    lanes_within_bundle = entry_matrix_inphase.shape[2]
    tok_local = lane_source_signal.shape[1]
    bundled_signal = lane_source_signal.astype(f32).reshape(
        groups_here, lanes_within_bundle, tok_local
    )
    step_size = jnp.exp(interval_exponent)[:, None]
    natural_pace_exponent = spectral_damping_part * step_size
    angle = spectral_angular_part * step_size
    num_re = jnp.expm1(natural_pace_exponent) * jnp.cos(angle) - 2.0 * jnp.sin(0.5 * angle) ** 2
    num_im = jnp.exp(natural_pace_exponent) * jnp.sin(angle)
    denom = (
        spectral_damping_part * spectral_damping_part
        + spectral_angular_part * spectral_angular_part
    )
    fac_re = (num_re * spectral_damping_part + num_im * spectral_angular_part) / denom
    fac_im = (num_im * spectral_damping_part - num_re * spectral_angular_part) / denom
    map_re = (
        fac_re[:, :, None] * entry_matrix_inphase - fac_im[:, :, None] * entry_matrix_quadrature
    )
    map_im = (
        fac_re[:, :, None] * entry_matrix_quadrature + fac_im[:, :, None] * entry_matrix_inphase
    )
    drive_re = jnp.einsum("gpc,gct->gpt", map_re, bundled_signal, precision=PRECISE_MODE)
    drive_im = jnp.einsum("gpc,gct->gpt", map_im, bundled_signal, precision=PRECISE_MODE)
    recurrence_modulus = jnp.exp(
        natural_pace_exponent[:, :, None] + spike_shrink_offset[:, None, :]
    )
    trans_re = recurrence_modulus * jnp.cos(angle)[:, :, None]
    trans_im = recurrence_modulus * jnp.sin(angle)[:, :, None]
    cum_re, cum_im, state_real, state_imaginary = local_prefix(
        (trans_re, trans_im, drive_re, drive_im)
    )
    summary = jnp.stack(
        [
            plane[:, :, -1].reshape(-1, 128)
            for plane in (cum_re, cum_im, state_real, state_imaginary)
        ]
    )
    entering = carry_call(summary)
    enter_re = entering[0].reshape(groups_here, -1)[:, :, None]
    enter_im = entering[1].reshape(groups_here, -1)[:, :, None]
    state_real = state_real + cum_re * enter_re - cum_im * enter_im
    state_imaginary = state_imaginary + cum_re * enter_im + cum_im * enter_re
    value = (
        jnp.einsum("nef,nfi->nei", emission_inphase, state_real, precision=PRECISE_MODE)
        - jnp.einsum("nef,nfi->nei", emission_quadrature, state_imaginary, precision=PRECISE_MODE)
        + lane_bypass_factor.reshape(groups_here, lanes_within_bundle)[:, :, None] * bundled_signal
    )
    recurrence_result = (
        jax.nn.gelu(value).astype(bf16).reshape(groups_here * lanes_within_bundle, tok_local)
    )
    share = dispatcher_scores / jnp.sum(dispatcher_scores, axis=1, keepdims=True)
    experts = lax.axis_size("sp")
    top = selected_specialists.shape[1]
    capacity = 2 * tok_local * top // experts
    flat_routes = selected_specialists.reshape(-1)
    hits = (flat_routes[:, None] == jnp.arange(experts, dtype=jnp.int32)[None, :]).astype(jnp.int32)
    ranks = jnp.sum((jnp.cumsum(hits, axis=0) - hits) * hits, axis=1)
    slot_ids = (flat_routes * capacity + ranks).reshape(tok_local, top)
    slot_grid = jnp.arange(experts * capacity, dtype=jnp.int32)
    pick = jnp.stack(
        [(slot_ids[:, k : k + 1] == slot_grid[None, :]).astype(bf16) for k in range(top)]
    )
    hot = jnp.any(slot_grid[:, None, None] == slot_ids.T[None, :, :], axis=1).astype(bf16)
    stream, rows = dispatch_call(
        recurrence_result.T,
        lane_exit_matrix,
        skipline_stream,
        specialist_scaling_vector[None, :],
        hot,
    )
    gate_part = jnp.dot(rows, specialist_valve_matrix[0], preferred_element_type=f32)
    up_part = jnp.dot(rows, specialist_widen_matrix[0], preferred_element_type=f32)
    hidden = (jax.nn.silu(gate_part) * up_part).astype(bf16)
    moe = return_call(hidden, specialist_shrink_matrix[0], share, pick)
    return (stream.astype(f32) + moe).astype(bf16)


def solution(mesh):
    placed = (
        P("tp", "sp"),
        P("tp", None),
        P("tp", None),
        P("tp"),
        P("tp", None, None),
        P("tp", None, None),
        P("tp", None, None),
        P("tp", None, None),
        P("tp"),
        P("tp", "sp"),
        P("tp", None),
        P("sp", None),
        P(),
        P("sp", None),
        P("sp", None),
        P("sp", None, "tp"),
        P("sp", None, "tp"),
        P("sp", "tp", None),
    )
    return jax.shard_map(
        per_device, mesh=mesh, in_specs=placed, out_specs=P("sp", "tp"), check_vma=False
    )
```

profile of v0, /device:TPU:0, one launch (start us, length us, event | category | flops | bytes accessed | tf_op | source)
XLA Modules:
  0.0 139.6 jit_solution(9612411070828648498)
XLA Ops:
  0.0 0.7 exp.13
  0.7 0.9 fusion.54
  1.6 1.6 %fusion.40 = f32[16,64,128]{2,1,0:T(8,128)S(1)} fusion(bf16[16,16,128]{2,1,0:T(8,128)(2,1)} %bitcast.113, f32[16,64,16]{1,2,0:T(8,128)} %param.22, f32[16,64,16]{1,2,0:T(8,128)} %param.23, f32[16,64]{1,0:T(8,128)S(1)} %get-tuple-element.35, f32[16,64]{1,0:T(8,128)S(1)} %get-tuple-element.34), kind=kOutput, calls=%fused_computation.72 | convolution fusion | flops 25214976 | bytes 729088 | tf_op jit(solution)/shard_map/gpc,gct->gpt/dot_general | solution.py:465
  3.2 1.6 %fusion.44 = f32[16,64,128]{2,1,0:T(8,128)S(1)} fusion(bf16[16,16,128]{2,1,0:T(8,128)(2,1)} %bitcast.114, f32[16,64,16]{1,2,0:T(8,128)} %param.23, f32[16,64,16]{1,2,0:T(8,128)} %param.22, f32[16,64]{1,0:T(8,128)S(1)} %get-tuple-element.35, f32[16,64]{1,0:T(8,128)S(1)} %get-tuple-element.34), kind=kOutput, calls=%fused_computation.76 | convolution fusion | flops 25214976 | bytes 729088 | tf_op jit(solution)/shard_map/gpc,gct->gpt/dot_general | solution.py:464
  4.8 1.5 %subtract_add_fusion.6 = (f32[16,64,128]{2,1,0:T(8,128)S(1)}, f32[16,64,128]{2,1,0:T(8,128)S(1)}, f32[16,64,128]{2,1,0:T(8,128)S(1)}, f32[16,64,128]{2,1,0:T(8,128)S(1)}) fusion(f32[16,64,128]{2,1,0:T(8,128)S(1)} %fusion.44, f32[16,64,127]{2,1,0:T(8,128)S(1)} %bitcast.109, f32[16,64,127]{2,1,0:T(8,128)S(1)} %bitcast.110, f32[16,64]{1,0:T(8,128)S(1)} %get-tuple-element.38, ...), kind=kLoop, calls=%fused_computation.40 | loop fusion | flops 1441792 | bytes 4206592 | tf_op jit(solution)/shard_map/add | solution.py:394
  6.2 1.0 add_add_fusion.5
  11.7 1.4 %add_add_fusion = (f32[16,64,128]{2,1,0:T(8,128)}, f32[16,64,128]{2,1,0:T(8,128)S(1)}, f32[16,64,128]{2,1,0:T(8,128)S(1)}) fusion(f32[16,64,128]{2,1,0:T(8,128)S(1)} %get-tuple-element.12, f32[16,64,64]{2,1,0:T(8,128)S(1)} %bitcast.73, f32[16,64,64]{2,1,0:T(8,128)S(1)} %bitcast.75, f32[16,64,128]{2,1,0:T(8,128)S(1)} %get-tuple-element.13, ...), kind=kLoop, calls=%fused_computation.24 | loop fusion | flops 1310720 | bytes 4456448 | tf_op jit(solution)/shard_map/add | solution.py:395
  13.1 1.4 %multiply_subtract_fusion = (f32[16,64,128]{2,1,0:T(8,128)}, f32[16,64,128]{2,1,0:T(8,128)S(1)}, f32[16,64,128]{2,1,0:T(8,128)S(1)}) fusion(f32[16,64,128]{2,1,0:T(8,128)S(1)} %get-tuple-element.10, f32[16,64,128]{2,1,0:T(8,128)S(1)} %get-tuple-element.11, f32[16,64,64]{2,1,0:T(8,128)S(1)} %bitcast.107, f32[16,64,64]{2,1,0:T(8,128)S(1)} %bitcast.108, ...), kind=kLoop, calls=%fused_computation.26 | loop fusion | flops 1310720 | bytes 4194304 | tf_op jit(solution)/shard_map/sub | solution.py:392
  14.6 0.8 copy-done.7
  16.1 1.4 %slice_reduce_fusion.3 = f32[16,64]{1,0:T(8,128)S(1)} fusion(f32[16,64,128]{2,1,0:T(8,128)} %get-tuple-element.27), kind=kLoop, calls=%fused_computation.12 | loop fusion | bytes 8192 | tf_op jit(solution)/shard_map/slice | solution.py:476
  17.7 1.4 %slice_reduce_fusion = f32[16,64]{1,0:T(8,128)S(1)} fusion(f32[16,64,128]{2,1,0:T(8,128)} %get-tuple-element.9), kind=kLoop, calls=%fused_computation.9 | loop fusion | bytes 8192 | tf_op jit(solution)/shard_map/slice | solution.py:476
  19.8 10.6 %carry.1 = f32[2,8,128]{2,1,0:T(8,128)} custom-call(f32[4,8,128]{2,1,0:T(8,128)} %pad_maximum_fusion.mine), custom_call_target="tpu_custom_call" | custom-call | tf_op jit(solution)/shard_map/carry/pallas_call | solution.py:64
  30.4 0.7 fusion.56
  31.2 2.2 %fusion.16 = f32[16,128,16]{1,2,0:T(8,128)S(1)} fusion(f32[16,16,64]{2,1,0:T(8,128)S(1)} %copy-done, f32[16,64,128]{2,1,0:T(8,128)} %copy-done.7, f32[16,64,128]{2,1,0:T(8,128)} %copy-done.8, f32[16,64,128]{2,1,0:T(8,128)} %get-tuple-element.27, f32[16,64]{1,0:T(8,128)S(1)} %mul.426, f32[16,64]{1,0:T(8,128)S(1)} %mul.423), kind=kOutput, calls=%fused_computation.19 | convolution fusion | flops 25690112 | bytes 1777664 | tf_op jit(solution)/shard_map/nef,nfi->nei/dot_general | solution.py:486
  34.1 2.2 %fusion.37 = bf16[16,16,128]{2,1,0:T(8,128)(2,1)S(1)} fusion(f32[16,128,16]{1,2,0:T(8,128)S(1)} %fusion.16, f32[16,16,64]{2,1,0:T(8,128)} %param.25, f32[16,64,128]{2,1,0:T(8,128)} %copy-done.7, f32[16,64,128]{2,1,0:T(8,128)} %get-tuple-element.9, f32[16,64,128]{2,1,0:T(8,128)} %get-tuple-element.27, f32[16,64]{1,0:T(8,128)} %copy-done.11, ...), kind=kOutput, calls=%fused_computation.71 | convolution fusion | flops 26116096 | bytes 1909760 | tf_op jit(solution)/shard_map/nef,nfi->nei/dot_general | solution.py:487
  36.5 0.8 copy.43
  37.4 0.8 reduce-window.6
  38.9 0.7 multiply_add_fusion.8
  39.7 49.5 %dispatch.1 = (bf16[128,1024]{1,0:T(8,128)(2,1)S(1)}, bf16[512,4096]{1,0:T(8,128)(2,1)S(1)}) custom-call(bf16[128,256]{1,0:T(8,128)(2,1)S(1)} %bitcast.71, bf16[256,4096]{1,0:T(8,128)(2,1)S(1)} %copy-done.2, bf16[128,4096]{1,0:T(8,128)(2,1)S(1)} %copy-done.3, f32[1,4096]{1,0:T(1,128)S(1)} %bitcast.72, bf16[512,128]{1,0:T(8,128)(2,1)S(1)} %convert_element_type.42.hot), custom_call_target="tpu_custom_call" | custom-call | tf_op jit(solution)/shard_map/dispatch/pallas_call | solution.py:231
  89.3 4.7 %fusion.2 = f32[512,512]{1,0:T(8,128)S(1)} fusion(bf16[512,4096]{1,0:T(8,128)(2,1)S(1)} %get-tuple-element.8, bf16[1,4096,512]{2,1,0:T(8,128)(2,1)} %param.33), kind=kOutput, calls=%fused_computation.2 | convolution fusion | flops 2147483648 | bytes 9437184 | tf_op jit(solution)/shard_map/dot_general | solution.py:513
  94.0 2.4 %fusion.7.hidden = bf16[512,512]{1,0:T(8,128)(2,1)S(1)} fusion(bf16[512,4096]{1,0:T(8,128)(2,1)S(1)} %get-tuple-element.8, bf16[1,4096,512]{2,1,0:T(8,128)(2,1)S(1)} %copy-done.15, f32[512,512]{1,0:T(8,128)S(1)} %fusion.2), kind=kOutput, calls=%fused_computation.5 | convolution fusion | flops 2149056512 | bytes 9961472 | tf_op jit(solution)/shard_map/dot_general | solution.py:514
  96.9 2.2 %copy-done.1 = bf16[1,512,4096]{2,1,0:T(8,128)(2,1)S(1)} copy-done((bf16[1,512,4096]{2,1,0:T(8,128)(2,1)S(1)}, bf16[1,512,4096]{2,1,0:T(8,128)(2,1)}, u32[]{:S(2)}) %copy-start.1) | copy-done | bytes 4194328
  99.1 39.7 %combine.1 = f32[128,1024]{1,0:T(8,128)S(1)} custom-call(bf16[512,512]{1,0:T(8,128)(2,1)S(1)} %fusion.7.hidden, bf16[512,4096]{1,0:T(8,128)(2,1)S(1)} %bitcast.70, f32[128,2]{1,0:T(8,128)S(1)} %broadcast_divide_fusion.share, bf16[2,128,512]{2,1,0:T(8,128)(2,1)S(1)} %add_convert_fusion.1.pick), custom_call_target="tpu_custom_call" | custom-call | tf_op jit(solution)/shard_map/combine/pallas_call | solution.py:364
  138.8 0.8 add_convert_fusion
  (66 shorter events, 8.2 us)
Async XLA Ops:
  0.0 31.2 %copy-start = (f32[16,16,64]{2,1,0:T(8,128)S(1)}, f32[16,16,64]{2,1,0:T(8,128)}, u32[]{:S(2)}) copy-start(f32[16,16,64]{2,1,0:T(8,128)} %param.24) | copy-start | bytes 196612
  0.0 6.2 %copy-start.12 = (f32[16,128]{1,0:T(8,128)S(1)}, f32[16,128]{1,0:T(8,128)}, u32[]{:S(2)}) copy-start(f32[16,128]{1,0:T(8,128)} %param.27) | copy-start | bytes 24580
  13.1 20.3 %copy-start.14 = (f32[256]{0:T(256)S(1)}, f32[256]{0:T(256)}, u32[]{:S(2)}) copy-start(f32[256]{0:T(256)} %param.26) | copy-start | bytes 3076
  13.1 21.0 %copy-start.9 = (bf16[256,128]{1,0:T(8,128)(2,1)S(1)}, bf16[256,128]{1,0:T(8,128)(2,1)}, u32[]{:S(2)}) copy-start(bf16[256,128]{1,0:T(8,128)(2,1)} %param.18) | copy-start | bytes 196612
  14.5 0.8 copy-start.7
  14.5 1.5 %copy-start.8 = (f32[16,64,128]{2,1,0:T(8,128)}, f32[16,64,128]{2,1,0:T(8,128)S(1)}, u32[]{:S(2)}) copy-start(f32[16,64,128]{2,1,0:T(8,128)S(1)} %get-tuple-element.31) | copy-start | bytes 1572868
  14.5 25.1 %copy-start.2 = (bf16[256,4096]{1,0:T(8,128)(2,1)S(1)}, bf16[256,4096]{1,0:T(8,128)(2,1)}, u32[]{:S(2)}) copy-start(bf16[256,4096]{1,0:T(8,128)(2,1)} %w.1) | copy-start | bytes 6291460
  14.5 25.2 %copy-start.3 = (bf16[128,4096]{1,0:T(8,128)(2,1)S(1)}, bf16[128,4096]{1,0:T(8,128)(2,1)}, u32[]{:S(2)}) copy-start(bf16[128,4096]{1,0:T(8,128)(2,1)} %skip.1) | copy-start | bytes 3145732
  14.5 25.2 %copy-start.6 = (f32[4096]{0:T(1024)S(1)}, f32[4096]{0:T(1024)}, u32[]{:S(2)}) copy-start(f32[4096]{0:T(1024)} %param.30) | copy-start | bytes 49156
  31.2 2.2 %copy-start.10 = (f32[16,64]{1,0:T(8,128)}, f32[16,64]{1,0:T(8,128)S(1)}, u32[]{:S(2)}) copy-start(f32[16,64]{1,0:T(8,128)S(1)} %mul.423) | copy-start | bytes 12292
  31.2 2.2 %copy-start.11 = (f32[16,64]{1,0:T(8,128)}, f32[16,64]{1,0:T(8,128)S(1)}, u32[]{:S(2)}) copy-start(f32[16,64]{1,0:T(8,128)S(1)} %mul.426) | copy-start | bytes 12292
  89.3 4.7 %copy-start.4 = (bf16[128,1024]{1,0:T(8,128)(2,1)}, bf16[128,1024]{1,0:T(8,128)(2,1)S(1)}, u32[]{:S(2)}) copy-start(bf16[128,1024]{1,0:T(8,128)(2,1)S(1)} %get-tuple-element.7) | copy-start | bytes 786436
  89.3 4.7 %copy-start.15 = (bf16[1,4096,512]{2,1,0:T(8,128)(2,1)S(1)}, bf16[1,4096,512]{2,1,0:T(8,128)(2,1)}, u32[]{:S(2)}) copy-start(bf16[1,4096,512]{2,1,0:T(8,128)(2,1)} %param.34) | copy-start | bytes 12582916
  94.0 2.7 %copy-start.13 = (f32[128,2]{0,1:T(2,128)S(1)}, f32[128,2]{0,1:T(2,128)}, u32[]{:S(2)}) copy-start(f32[128,2]{0,1:T(2,128)} %param.32) | copy-start | bytes 3076
  96.4 42.4 %copy-start.5 = (bf16[128,1024]{1,0:T(8,128)(2,1)S(1)}, bf16[128,1024]{1,0:T(8,128)(2,1)}, u32[]{:S(2)}) copy-start(bf16[128,1024]{1,0:T(8,128)(2,1)} %copy-done.4) | copy-start | bytes 786436
  96.9 2.2 %copy-start.1 = (bf16[1,512,4096]{2,1,0:T(8,128)(2,1)S(1)}, bf16[1,512,4096]{2,1,0:T(8,128)(2,1)}, u32[]{:S(2)}) copy-start(bf16[1,512,4096]{2,1,0:T(8,128)(2,1)} %param.35) | copy-start | bytes 12582916
where the time goes:
time: 141 us; the launch traced here: 140 us
  Pallas kernels  99.9 us (71%)
  matrix products  14.7 us (10%)
  other arithmetic  13.9 us (10%)
  local copies, waits for them, and re-layouts  10.7 us (8%)
    pallas_call x1, Pallas kernels, dispatch_call(): pl.pallas_call(dispatch_kernel, out_shape=(jax.ShapeDtypeStruct((tok, d_l...  49.5 us
    pallas_call x1, Pallas kernels, return_call(): pl.pallas_call(return_kernel, out_shape=jax.ShapeDtypeStruct((tok, d_loca...  39.7 us
    pallas_call x1, Pallas kernels, carry_call(): pl.pallas_call(carry_kernel, out_shape=jax.ShapeDtypeStruct((2,) + summar...  10.6 us
    add x6, other arithmetic, affine_pair(): add_im = latter[0] * earlier[3] + latter[1] * earlier[2] + latter[3]  4.89 us
    dot_general x1, matrix products, per_device(): jnp.dot(rows, specialist_valve_matrix[0], preferred_element_type=f32)  4.66 us
    unnamed x34, local copies, waits for them, and re-layouts  3.94 us
    slice x3, local copies, waits for them, and re-layouts, per_device(): plane[:, :, -1].reshape(-1, 128)  3.5 us
    add x6, other arithmetic, affine_pair(): add_re = latter[0] * earlier[2] - latter[1] * earlier[3] + latter[2]  3.41 us

commit v1 on v0

--- a/solution.py
+++ b/solution.py
@@ -6,7 +6,6 @@
 from jax.sharding import PartitionSpec as P
 
 EPS = 1e-06
-PRECISE_MODE = lax.Precision.HIGHEST
 
 
 MESH = pl.DeviceIdType.MESH
@@ -33,19 +32,186 @@
     return n_sp, n_tp, lax.axis_index("sp"), lax.axis_index("tp")
 
 
-def carry_kernel(mine, out, pieces, send, recv):
+def tp_peers(n_tp, me, lane):
+    return [(me, lax.rem(lane + i, n_tp)) for i in range(1, n_tp)]
+
+
+def sp_peers(n_sp, me, lane):
+    return [(lax.rem(me + i, n_sp), lane) for i in range(1, n_sp)]
+
+
+def affine_pair(earlier, latter):
+    mul_re = earlier[0] * latter[0] - earlier[1] * latter[1]
+    mul_im = earlier[0] * latter[1] + earlier[1] * latter[0]
+    add_re = latter[0] * earlier[2] - latter[1] * earlier[3] + latter[2]
+    add_im = latter[0] * earlier[3] + latter[1] * earlier[2] + latter[3]
+    return (mul_re, mul_im, add_re, add_im)
+
+
+def dot_nt(a, b, precision=None):
+    return lax.dot_general(
+        a, b, (((1,), (1,)), ((), ())), precision=precision, preferred_element_type=jnp.float32
+    )
+
+
+def iota(shape, dim):
+    return lax.broadcasted_iota(jnp.int32, shape, dim)
+
+
+def expm1_of(x):
+    series = jnp.ones_like(x)
+    for k in range(11, 1, -1):
+        series = 1.0 + x * series * (1.0 / k)
+    return jnp.where(jnp.abs(x) < 0.7, x * series, jnp.exp(x) - 1.0)
+
+
+def mixer_kernel(
+    u, damp, ang, log_dt, ent_re, ent_im, emi_re, emi_im, bypass, shrink, sel, scores,
+    rows_out, hot_out, pick_out, share_out,
+    xr, xi, cr, ci, mine, pieces, send, recv,
+):
+    f32, bf16 = jnp.float32, jnp.bfloat16
     n_sp, n_tp, me, lane = places()
-    greet([(lax.rem(me + i, n_sp), lane) for i in range(1, n_sp)])
-    copies = []
-    for i in range(1, n_sp):
-        copy = remote(
+    barrier = pltpu.get_barrier_semaphore()
+    for peer in sp_peers(n_sp, me, lane):
+        pl.semaphore_signal(barrier, inc=1, device_id=peer, device_id_type=MESH)
+
+    groups, p_size = damp.shape
+    chans, tok = u.shape
+    gs = chans // groups
+    states = groups * p_size
+    tiles = states // 128
+    per = 128 // p_size
+    n_j = 8
+    n_i = tok // n_j
+
+    def lane_group(rows):
+        return iota((rows, 128), 1) // p_size
+
+    def as_row(a):
+        wide = jnp.concatenate([a] * per, axis=1)
+        parts = []
+        for tile in range(tiles):
+            row = wide[per * tile : per * tile + 1]
+            for k in range(1, per):
+                row = jnp.where(lane_group(1) == k, wide[per * tile + k : per * tile + k + 1], row)
+            parts.append(row)
+        return jnp.concatenate(parts, axis=1)
+
+    def spread(columns, tile):
+        out = jnp.broadcast_to(columns[:, per * tile : per * tile + 1], (tok, 128))
+        for k in range(1, per):
+            other = jnp.broadcast_to(columns[:, per * tile + k : per * tile + k + 1], (tok, 128))
+            out = jnp.where(lane_group(tok) == k, other, out)
+        return out
+
+    eye = (iota((groups, groups), 0) == iota((groups, groups), 1)).astype(f32)
+    dt = jnp.exp(jnp.sum(eye * log_dt[...], axis=1, keepdims=True))
+    a_re, a_im = damp[...], ang[...]
+    log_rate = a_re * dt
+    angle = a_im * dt
+    cos, sin = jnp.cos(angle), jnp.sin(angle)
+    half = jnp.sin(0.5 * angle)
+    decay = jnp.exp(log_rate)
+    num_re = expm1_of(log_rate) * cos - 2.0 * half * half
+    num_im = decay * sin
+    denom = a_re * a_re + a_im * a_im
+    fac_re = as_row((num_re * a_re + num_im * a_im) / denom)
+    fac_im = as_row((num_im * a_re - num_re * a_im) / denom)
+    lam_re = as_row(decay * cos)
+    lam_im = as_row(decay * sin)
+
+    order = iota((tok, tok), 0)
+    perm = ((order % n_j) * n_i + order // n_j == iota((tok, tok), 1)).astype(f32)
+    columns = jnp.exp(dot_nt(perm, shrink[...], lax.Precision.HIGHEST))
+    signal = dot_nt(perm.astype(bf16), u[...])
+    eye_c = (iota((gs, gs), 0) == iota((gs, gs), 1)).astype(f32)
+    in_re = dot_nt(eye_c, ent_re[...], lax.Precision.HIGHEST)
+    in_im = dot_nt(eye_c, ent_im[...], lax.Precision.HIGHEST)
+    same = iota((chans, states), 0) // gs == iota((chans, states), 1) // p_size
+
+    def block_rows(a):
+        return jnp.where(same, jnp.concatenate([a] * groups, axis=0), 0.0)
+
+    drive_re = jnp.dot(
+        signal, block_rows(fac_re * in_re - fac_im * in_im),
+        precision=lax.Precision.HIGH, preferred_element_type=f32,
+    )
+    drive_im = jnp.dot(
+        signal, block_rows(fac_re * in_im + fac_im * in_re),
+        precision=lax.Precision.HIGH, preferred_element_type=f32,
+    )
+    row_j = iota((n_j, 128), 0)
+    ends = []
+    for tile in range(tiles):
+        at = slice(128 * tile, 128 * tile + 128)
+        modulus = spread(columns, tile)
+        t_re, t_im = modulus * lam_re[:, at], modulus * lam_im[:, at]
+        for i in range(n_i):
+            step = slice(n_j * i, n_j * i + n_j)
+            now = (t_re[step], t_im[step], drive_re[step, at], drive_im[step, at])
+            run = now if i == 0 else affine_pair(run, now)
+            for ref, value in zip((cr, ci, xr, xi), run):
+                ref[step, at] = value
+        off = 1
+        while off < n_j:
+            before = [pltpu.roll(value, off, 0) for value in run]
+            joined = affine_pair(before, run)
+            run = tuple(jnp.where(row_j >= off, new, old) for new, old in zip(joined, run))
+            off *= 2
+        for plane in range(4):
+            mine[plane, tile : tile + 1, :] = run[plane][n_j - 1 : n_j]
+        fills = (1.0, 0.0, 0.0, 0.0)
+        ends.append(
+            [jnp.where(row_j >= 1, pltpu.roll(v, 1, 0), fill) for v, fill in zip(run, fills)]
+        )
+
+    pl.semaphore_wait(barrier, n_sp - 1)
+
+    def carry_copy(i):
+        return remote(
             mine, pieces.at[i - 1], send.at[i - 1], recv.at[i - 1], (lax.rem(me + i, n_sp), lane)
         )
-        copy.start()
-        copies.append(copy)
-    for copy in copies:
-        copy.wait_recv()
-    run_re = jnp.zeros(mine.shape[1:], jnp.float32)
+
+    for i in range(1, n_sp):
+        @pl.when(me + i < n_sp)
+        def _(i=i):
+            carry_copy(i).start()
+
+    share_out[...] = scores[...] / jnp.sum(scores[...], axis=1, keepdims=True)
+    top = sel.shape[1]
+    slots = hot_out.shape[0]
+    cap = slots // n_sp
+    choice = [sel[:, k : k + 1] == iota((tok, 128), 1) for k in range(top)]
+    member = choice[0]
+    for other in choice[1:]:
+        member = member | other
+    member = jnp.where(member, 1.0, 0.0)
+    below = jnp.where(iota((tok, tok), 1) <= iota((tok, tok), 0), 1.0, 0.0).astype(bf16)
+    rank = jnp.dot(below, member.astype(bf16), preferred_element_type=f32)
+    of_slot = jnp.where(iota((slots, 128), 0) // cap == iota((slots, 128), 1), 1.0, 0.0).astype(bf16)
+    code = (member * rank).astype(bf16)
+    want = (iota((slots, tok), 0) % cap + 1).astype(f32)
+    hot_out[...] = jnp.where(dot_nt(of_slot, code) == want, 1.0, 0.0).astype(bf16)
+    want = (iota((tok, slots), 1) % cap + 1).astype(f32)
+    for k in range(top):
+        mark = jnp.where(choice[k], rank, 0.0).astype(bf16)
+        pick_out[k] = jnp.where(dot_nt(mark, of_slot) == want, 1.0, 0.0).astype(bf16)
+
+    out_lane = iota((chans, states), 1) // p_size
+    out_row = iota((chans, states), 0) // gs
+
+    def block_cols(a):
+        wide = jnp.concatenate([a] * per, axis=1)
+        return jnp.where(out_row == out_lane, jnp.concatenate([wide] * tiles, axis=1), 0.0)
+
+    q_re, q_im = block_cols(emi_re[...]), block_cols(emi_im[...])
+
+    for i in range(1, n_sp):
+        @pl.when(me >= i)
+        def _(i=i):
+            carry_copy(i).wait_recv()
+    run_re = jnp.zeros(mine.shape[1:], f32)
     run_im = run_re
     for i in range(n_sp - 1, 0, -1):
         mul_re, mul_im, add_re, add_im = (pieces[i - 1, plane] for plane in range(4))
@@ -53,35 +219,65 @@
         new_im = mul_re * run_im + mul_im * run_re + add_im
         run_re = jnp.where(me >= i, new_re, run_re)
         run_im = jnp.where(me >= i, new_im, run_im)
-    out[0] = run_re
-    out[1] = run_im
-    for copy in copies:
-        copy.wait_send()
-
-
-def carry_call(summary):
+
+    for tile in range(tiles):
+        at = slice(128 * tile, 128 * tile + 128)
+        p_re, p_im, z_re, z_im = ends[tile]
+        e_re, e_im = run_re[tile : tile + 1], run_im[tile : tile + 1]
+        z_re = z_re + p_re * e_re - p_im * e_im
+        z_im = z_im + p_re * e_im + p_im * e_re
+        for i in range(n_i):
+            step = slice(n_j * i, n_j * i + n_j)
+            c_re, c_im = cr[step, at], ci[step, at]
+            xr[step, at] = xr[step, at] + c_re * z_re - c_im * z_im
+            xi[step, at] = xi[step, at] + c_re * z_im + c_im * z_re
+    value = (
+        dot_nt(xr[...], q_re, lax.Precision.HIGH)
+        - dot_nt(xi[...], q_im, lax.Precision.HIGH)
+        + signal * bypass[...]
+    )
+    mixed = jax.nn.gelu(value).astype(bf16)
+    order = iota((tok, tok), 1)
+    back = ((order % n_j) * n_i + order // n_j == iota((tok, tok), 0)).astype(bf16)
+    rows_out[...] = jnp.dot(back, mixed, preferred_element_type=f32).astype(bf16)
+
+    for i in range(1, n_sp):
+        @pl.when(me + i < n_sp)
+        def _(i=i):
+            carry_copy(i).wait_send()
+
+
+def mixer_call(u, damp, ang, log_dt, ent_re, ent_im, emi_re, emi_im, bypass, shrink, sel, scores):
     n_sp = lax.axis_size("sp")
+    f32, bf16 = jnp.float32, jnp.bfloat16
+    chans, tok = u.shape
+    groups, p_size = damp.shape
+    states = groups * p_size
+    top = sel.shape[1]
+    slots = 2 * tok * top
+    plane = (4, states // 128, 128)
     return pl.pallas_call(
-        carry_kernel,
-        out_shape=jax.ShapeDtypeStruct((2,) + summary.shape[1:], jnp.float32),
-        in_specs=[VM],
-        out_specs=VM,
-        scratch_shapes=[
-            pltpu.VMEM((n_sp - 1,) + summary.shape, jnp.float32),
+        mixer_kernel,
+        out_shape=(
+            jax.ShapeDtypeStruct((tok, chans), bf16),
+            jax.ShapeDtypeStruct((slots, tok), bf16),
+            jax.ShapeDtypeStruct((top, tok, slots), bf16),
+            jax.ShapeDtypeStruct((tok, top), f32),
+        ),
+        in_specs=[VM] * 12,
+        out_specs=(VM,) * 4,
+        scratch_shapes=[pltpu.VMEM((tok, states), f32)] * 4
+        + [
+            pltpu.VMEM(plane, f32),
+            pltpu.VMEM((n_sp - 1,) + plane, f32),
             DMA((n_sp - 1,)),
             DMA((n_sp - 1,)),
         ],
-        compiler_params=pltpu.CompilerParams(collective_id=0, has_side_effects=True),
-        name="carry",
-    )(summary)
-
-
-def tp_peers(n_tp, me, lane):
-    return [(me, lax.rem(lane + i, n_tp)) for i in range(1, n_tp)]
-
-
-def sp_peers(n_sp, me, lane):
-    return [(lax.rem(me + i, n_sp), lane) for i in range(1, n_sp)]
+        compiler_params=pltpu.CompilerParams(
+            collective_id=0, has_side_effects=True, vmem_limit_bytes=VMEM_ROOM // 2
+        ),
+        name="mixer",
+    )(u, damp, ang, log_dt, ent_re, ent_im, emi_re, emi_im, bypass, shrink, sel, scores)
 
 
 def dispatch_kernel(
@@ -388,34 +584,6 @@
     )(hidden, w, share, pick)
 
 
-def affine_pair(earlier, latter):
-    mul_re = earlier[0] * latter[0] - earlier[1] * latter[1]
-    mul_im = earlier[0] * latter[1] + earlier[1] * latter[0]
-    add_re = latter[0] * earlier[2] - latter[1] * earlier[3] + latter[2]
-    add_im = latter[0] * earlier[3] + latter[1] * earlier[2] + latter[3]
-    return (mul_re, mul_im, add_re, add_im)
-
-
-def local_prefix(elements):
-    length = elements[0].shape[2]
-    fills = (1.0, 0.0, 0.0, 0.0)
-    offset = 1
-    while offset < length:
-        earlier = tuple(
-            (
-                jnp.pad(
-                    item[:, :, : length - offset],
-                    ((0, 0), (0, 0), (offset, 0)),
-                    constant_values=fill,
-                )
-                for item, fill in zip(elements, fills)
-            )
-        )
-        elements = affine_pair(earlier, elements)
-        offset = offset * 2
-    return elements
-
-
 def per_device(
     lane_source_signal,
     spectral_damping_part,
@@ -436,75 +604,25 @@
     specialist_widen_matrix,
     specialist_shrink_matrix,
 ):
-    f32 = jnp.float32
-    bf16 = jnp.bfloat16
-    groups_here = spectral_damping_part.shape[0]
-    lanes_within_bundle = entry_matrix_inphase.shape[2]
-    tok_local = lane_source_signal.shape[1]
-    bundled_signal = lane_source_signal.astype(f32).reshape(
-        groups_here, lanes_within_bundle, tok_local
-    )
-    step_size = jnp.exp(interval_exponent)[:, None]
-    natural_pace_exponent = spectral_damping_part * step_size
-    angle = spectral_angular_part * step_size
-    num_re = jnp.expm1(natural_pace_exponent) * jnp.cos(angle) - 2.0 * jnp.sin(0.5 * angle) ** 2
-    num_im = jnp.exp(natural_pace_exponent) * jnp.sin(angle)
-    denom = (
-        spectral_damping_part * spectral_damping_part
-        + spectral_angular_part * spectral_angular_part
-    )
-    fac_re = (num_re * spectral_damping_part + num_im * spectral_angular_part) / denom
-    fac_im = (num_im * spectral_damping_part - num_re * spectral_angular_part) / denom
-    map_re = (
-        fac_re[:, :, None] * entry_matrix_inphase - fac_im[:, :, None] * entry_matrix_quadrature
-    )
-    map_im = (
-        fac_re[:, :, None] * entry_matrix_quadrature + fac_im[:, :, None] * entry_matrix_inphase
-    )
-    drive_re = jnp.einsum("gpc,gct->gpt", map_re, bundled_signal, precision=PRECISE_MODE)
-    drive_im = jnp.einsum("gpc,gct->gpt", map_im, bundled_signal, precision=PRECISE_MODE)
-    recurrence_modulus = jnp.exp(
-        natural_pace_exponent[:, :, None] + spike_shrink_offset[:, None, :]
-    )
-    trans_re = recurrence_modulus * jnp.cos(angle)[:, :, None]
-    trans_im = recurrence_modulus * jnp.sin(angle)[:, :, None]
-    cum_re, cum_im, state_real, state_imaginary = local_prefix(
-        (trans_re, trans_im, drive_re, drive_im)
-    )
-    summary = jnp.stack(
-        [
-            plane[:, :, -1].reshape(-1, 128)
-            for plane in (cum_re, cum_im, state_real, state_imaginary)
-        ]
-    )
-    entering = carry_call(summary)
-    enter_re = entering[0].reshape(groups_here, -1)[:, :, None]
-    enter_im = entering[1].reshape(groups_here, -1)[:, :, None]
-    state_real = state_real + cum_re * enter_re - cum_im * enter_im
-    state_imaginary = state_imaginary + cum_re * enter_im + cum_im * enter_re
-    value = (
-        jnp.einsum("nef,nfi->nei", emission_inphase, state_real, precision=PRECISE_MODE)
-        - jnp.einsum("nef,nfi->nei", emission_quadrature, state_imaginary, precision=PRECISE_MODE)
-        + lane_bypass_factor.reshape(groups_here, lanes_within_bundle)[:, :, None] * bundled_signal
-    )
-    recurrence_result = (
-        jax.nn.gelu(value).astype(bf16).reshape(groups_here * lanes_within_bundle, tok_local)
-    )
-    share = dispatcher_scores / jnp.sum(dispatcher_scores, axis=1, keepdims=True)
-    experts = lax.axis_size("sp")
-    top = selected_specialists.shape[1]
-    capacity = 2 * tok_local * top // experts
-    flat_routes = selected_specialists.reshape(-1)
-    hits = (flat_routes[:, None] == jnp.arange(experts, dtype=jnp.int32)[None, :]).astype(jnp.int32)
-    ranks = jnp.sum((jnp.cumsum(hits, axis=0) - hits) * hits, axis=1)
-    slot_ids = (flat_routes * capacity + ranks).reshape(tok_local, top)
-    slot_grid = jnp.arange(experts * capacity, dtype=jnp.int32)
-    pick = jnp.stack(
-        [(slot_ids[:, k : k + 1] == slot_grid[None, :]).astype(bf16) for k in range(top)]
-    )
-    hot = jnp.any(slot_grid[:, None, None] == slot_ids.T[None, :, :], axis=1).astype(bf16)
+    f32, bf16 = jnp.float32, jnp.bfloat16
+    gs = entry_matrix_inphase.shape[2]
+    p_size = spectral_damping_part.shape[1]
+    mixed, hot, pick, share = mixer_call(
+        lane_source_signal,
+        spectral_damping_part,
+        spectral_angular_part,
+        interval_exponent[None, :],
+        entry_matrix_inphase.reshape(-1, gs),
+        entry_matrix_quadrature.reshape(-1, gs),
+        emission_inphase.reshape(-1, p_size),
+        emission_quadrature.reshape(-1, p_size),
+        lane_bypass_factor[None, :],
+        spike_shrink_offset,
+        selected_specialists,
+        dispatcher_scores,
+    )
     stream, rows = dispatch_call(
-        recurrence_result.T,
+        mixed,
         lane_exit_matrix,
         skipline_stream,
         specialist_scaling_vector[None, :],

time: 141 us -> 121 us (0.86)
  other arithmetic: 13.9 us -> 0.76 us
  matrix products: 14.7 us -> 7.11 us
    add x13 -> x0, other arithmetic: 9 us -> none  [the longest x6 4.89 us: affine_pair(): add_im = latter[0] * earlier[3] + latter[1] * earlier[2] + latter[3]]
    unnamed x34 -> x30, local copies, waits for them, and re-layouts: 3.94 us -> 12 us
    dot_general x4 -> x0, matrix products: 7.55 us -> none  [the longest x1 2.23 us: per_device(): jnp.einsum('nef,nfi->nei', emission_quadrature, state_imaginary, precisio...]
    slice x5 -> x0, local copies, waits for them, and re-layouts: 4.4 us -> none  [the longest x3 3.5 us: per_device(): plane[:, :, -1].reshape(-1, 128)]
    pallas_call x1, Pallas kernels: 10.6 us -> 8.35 us  [mixer_call(): pl.pallas_call(mixer_kernel, out_shape=(jax.ShapeDtypeStruct((tok, chans)...]
    pallas_call x1, Pallas kernels: 49.5 us -> 51.5 us  [dispatch_call(): pl.pallas_call(dispatch_kernel, out_shape=(jax.ShapeDtypeStruct((tok, d_l...]
    another operation x4 -> x0, other arithmetic: 1.44 us -> none
    sub x1 -> x0, other arithmetic: 1.42 us -> none  [affine_pair(): mul_re = earlier[0] * latter[0] - earlier[1] * latter[1]]
where the time goes in v1:
time: 121 us; the launch traced here: 120 us
  Pallas kernels  99.7 us (82%)
  local copies, waits for them, and re-layouts  12 us (10%)
  matrix products  7.11 us (6%)
    pallas_call x1, Pallas kernels, dispatch_call(): pl.pallas_call(dispatch_kernel, out_shape=(jax.ShapeDtypeStruct((tok, d_l...  51.5 us
    pallas_call x1, Pallas kernels, return_call(): pl.pallas_call(return_kernel, out_shape=jax.ShapeDtypeStruct((tok, d_loca...  39.8 us
    unnamed x30, local copies, waits for them, and re-layouts  12 us
    pallas_call x1, Pallas kernels, mixer_call(): pl.pallas_call(mixer_kernel, out_shape=(jax.ShapeDtypeStruct((tok, chans)...  8.35 us
    dot_general x1, matrix products, per_device(): jnp.dot(rows, specialist_valve_matrix[0], preferred_element_type=f32)  4.66 us
    dot_general x1, matrix products, per_device(): jnp.dot(rows, specialist_widen_matrix[0], preferred_element_type=f32)  2.45 us

profile of v1, /device:TPU:0, one launch (start us, length us, event | category | flops | bytes accessed | tf_op | source)
XLA Modules:
  0.0 119.6 jit_solution(4422130408286615879)
XLA Ops:
  0.0 0.9 copy.21.sel
  0.9 0.8 copy.22.scores
  1.7 1.1 copy.19
  2.8 1.1 copy.20
  3.9 0.0 copy-start.3
  4.0 0.9 copy-done.3
  4.9 0.9 copy-done.4
  5.8 0.8 copy-done.5
  6.6 0.7 copy-done.7
  7.3 0.7 copy-done.8
  8.0 0.7 copy-done.9
  8.7 0.7 copy-done.10
  9.4 0.7 copy-done.11
  10.0 8.3 %mixer.1 = (bf16[128,256]{1,0:T(8,128)(2,1)S(1)}, bf16[512,128]{1,0:T(8,128)(2,1)S(1)}, bf16[2,128,512]{2,1,0:T(8,128)(2,1)S(1)}, f32[128,2]{1,0:T(8,128)S(1)}) custom-call(bf16[256,128]{1,0:T(8,128)(2,1)S(1)} %copy-done.5, f32[16,64]{1,0:T(8,128)S(1)} %copy-done.7, f32[16,64]{1,0:T(8,128)S(1)} %copy-done.8, f32[1,16]{1,0:T(1,128)S(1)} %bitcast.27, ...), custom_call_target="tpu_custom_call" | custom-call | tf_op jit(solution)/shard_map/mixer/pallas_call | solution.py:259
  18.4 0.0 copy-start.2
  18.4 1.2 %copy-done.2 = bf16[128,4096]{1,0:T(8,128)(2,1)S(1)} copy-done((bf16[128,4096]{1,0:T(8,128)(2,1)S(1)}, bf16[128,4096]{1,0:T(8,128)(2,1)}, u32[]{:S(2)}) %copy-start.2) | copy-done | bytes 1048600
  19.6 0.7 copy-done.6
  20.3 51.5 %dispatch.1 = (bf16[128,1024]{1,0:T(8,128)(2,1)S(1)}, bf16[512,4096]{1,0:T(8,128)(2,1)S(1)}) custom-call(bf16[128,256]{1,0:T(8,128)(2,1)S(1)} %get-tuple-element.11.rows, bf16[256,4096]{1,0:T(8,128)(2,1)S(1)} %copy-done.1, bf16[128,4096]{1,0:T(8,128)(2,1)S(1)} %copy-done.2, f32[1,4096]{1,0:T(1,128)S(1)} %bitcast.25, bf16[512,128]{1,0:T(8,128)(2,1)S(1)} %get-tuple-element.12.hot), custom_call_target="tpu_custom_call" | custom-call | tf_op jit(solution)/shard_map/dispatch/pallas_call | solution.py:427
  71.9 0.0 copy-start.12
  71.9 4.7 %fusion.2 = f32[512,512]{1,0:T(8,128)S(1)} fusion(bf16[512,4096]{1,0:T(8,128)(2,1)S(1)} %get-tuple-element.14, bf16[1,4096,512]{2,1,0:T(8,128)(2,1)} %param.33), kind=kOutput, calls=%fused_computation.2 | convolution fusion | flops 2147483648 | bytes 9437184 | tf_op jit(solution)/shard_map/dot_general | solution.py:631
  76.6 0.0 copy-start
  76.6 2.5 %fusion.7.hidden = bf16[512,512]{1,0:T(8,128)(2,1)S(1)} fusion(bf16[512,4096]{1,0:T(8,128)(2,1)S(1)} %get-tuple-element.14, bf16[1,4096,512]{2,1,0:T(8,128)(2,1)S(1)} %copy-done.12, f32[512,512]{1,0:T(8,128)S(1)} %fusion.2), kind=kOutput, calls=%fused_computation.5 | convolution fusion | flops 2149056512 | bytes 9961472 | tf_op jit(solution)/shard_map/dot_general | solution.py:632
  79.0 39.8 %combine.1 = f32[128,1024]{1,0:T(8,128)S(1)} custom-call(bf16[512,512]{1,0:T(8,128)(2,1)S(1)} %fusion.7.hidden, bf16[512,4096]{1,0:T(8,128)(2,1)S(1)} %bitcast.20, f32[128,2]{1,0:T(8,128)S(1)} %get-tuple-element.15.share, bf16[2,128,512]{2,1,0:T(8,128)(2,1)S(1)} %get-tuple-element.16.pick), custom_call_target="tpu_custom_call" | custom-call | tf_op jit(solution)/shard_map/combine/pallas_call | solution.py:560
  118.9 0.8 add_convert_fusion
  (12 shorter events, 0.0 us)
Async XLA Ops:
  0.0 18.4 %copy-start.1 = (bf16[256,4096]{1,0:T(8,128)(2,1)S(1)}, bf16[256,4096]{1,0:T(8,128)(2,1)}, u32[]{:S(2)}) copy-start(bf16[256,4096]{1,0:T(8,128)(2,1)} %w.1) | copy-start | bytes 6291460
  3.9 0.9 copy-start.3
  4.9 0.9 copy-start.4
  5.8 0.8 copy-start.5
  6.6 0.7 copy-start.7
  7.3 0.7 copy-start.8
  8.0 0.7 copy-start.9
  8.7 0.7 copy-start.10
  9.4 0.7 copy-start.11
  18.4 1.2 %copy-start.2 = (bf16[128,4096]{1,0:T(8,128)(2,1)S(1)}, bf16[128,4096]{1,0:T(8,128)(2,1)}, u32[]{:S(2)}) copy-start(bf16[128,4096]{1,0:T(8,128)(2,1)} %skip.1) | copy-start | bytes 3145732
  19.6 0.7 copy-start.6
  71.9 4.7 %copy-start.12 = (bf16[1,4096,512]{2,1,0:T(8,128)(2,1)S(1)}, bf16[1,4096,512]{2,1,0:T(8,128)(2,1)}, u32[]{:S(2)}) copy-start(bf16[1,4096,512]{2,1,0:T(8,128)(2,1)} %param.34) | copy-start | bytes 12582916
  76.6 2.5 %copy-start = (bf16[1,512,4096]{2,1,0:T(8,128)(2,1)S(1)}, bf16[1,512,4096]{2,1,0:T(8,128)(2,1)}, u32[]{:S(2)}) copy-start(bf16[1,512,4096]{2,1,0:T(8,128)(2,1)} %param.35) | copy-start | bytes 12582916

commit v2 on v1

v2 whole, which is shorter than its diff:
```python
import jax
import jax.numpy as jnp
from jax import lax
from jax.experimental import pallas as pl
from jax.experimental.pallas import tpu as pltpu
from jax.sharding import PartitionSpec as P

EPS = 1e-06
MESH = pl.DeviceIdType.MESH
VM = pl.BlockSpec(memory_space=pltpu.VMEM)
FAR = pl.BlockSpec(memory_space=pl.ANY)
DMA = pltpu.SemaphoreType.DMA
VMEM_ROOM = 60 * 1024 * 1024
HIGH, HIGHEST = lax.Precision.HIGH, lax.Precision.HIGHEST
GROUP = 128


def remote(src, dst, send, recv, where):
    return pltpu.make_async_remote_copy(
        src_ref=src, dst_ref=dst, send_sem=send, recv_sem=recv, device_id=where, device_id_type=MESH
    )


def places():
    n_sp, n_tp = lax.axis_size("sp"), lax.axis_size("tp")
    return n_sp, n_tp, lax.axis_index("sp"), lax.axis_index("tp")


def xor(a, b, n):
    out, bit = 0, 1
    while bit < n:
        p, q = lax.rem(lax.div(a, bit), 2), (b // bit) % 2
        out = out + bit * (p + q - 2 * p * q)
        bit *= 2
    return out


def dot(a, b, precision=None):
    return jnp.dot(a, b, precision=precision, preferred_element_type=jnp.float32)


def dot_nt(a, b, precision=None):
    return lax.dot_general(
        a, b, (((1,), (1,)), ((), ())), precision=precision, preferred_element_type=jnp.float32
    )


def iota(shape, dim):
    return lax.broadcasted_iota(jnp.int32, shape, dim)


def where_one(mask):
    return jnp.where(mask, 1.0, 0.0)


def expm1_of(x):
    series = jnp.ones_like(x)
    for k in range(11, 1, -1):
        series = 1.0 + x * series * (1.0 / k)
    return jnp.where(jnp.abs(x) < 0.7, x * series, jnp.exp(x) - 1.0)


def affine_pair(earlier, latter):
    mul_re = earlier[0] * latter[0] - earlier[1] * latter[1]
    mul_im = earlier[0] * latter[1] + earlier[1] * latter[0]
    add_re = latter[0] * earlier[2] - latter[1] * earlier[3] + latter[2]
    add_im = latter[0] * earlier[3] + latter[1] * earlier[2] + latter[3]
    return (mul_re, mul_im, add_re, add_im)


N_IN = 18


def layer_kernel(*refs):
    f32, bf16 = jnp.float32, jnp.bfloat16
    far = refs[:N_IN]
    out = refs[N_IN]
    near = refs[N_IN + 1 : 2 * N_IN + 1]
    (
        fetched, xr, xi, cr, ci, mine, pieces, mixed_s, hot, weigh, stream_s,
        psend_a, precv_a, ysend_a, yrecv_a, ssend, srecv,
        xs, dsend, psend, own, precv, ysend, yrecv, rsend, ret,
        carry_s, carry_r, pa_s, pa_r, ya_s, ya_r, sum_s, sum_r, d_s, d_r,
        f_s, f_r, q_s, q_r, p_s, p_r, y_s, y_r, r_s, r_r,
    ) = refs[2 * N_IN + 1 :]
    (
        u, damp, ang, log_dt, ent_re, ent_im, emi_re, emi_im, bypass, shrink, sel, scores,
        w, skip, gain, wg, wu, wd,
    ) = near
    n_sp, n_tp, me, lane = places()
    n_y = n_tp // 2
    y, core = lax.div(lane, 2), lax.rem(lane, 2)
    partner = (me, y * 2 + 1 - core)
    tok, d_local = out.shape
    slots, width = xs.shape
    cap = slots // n_sp
    per_group = GROUP // cap
    n_groups = slots // GROUP

    def cols(block):
        return pl.ds(pl.multiple_of(block * d_local, 128), d_local)

    def peer(k):
        return (xor(me, k, n_sp), lane)

    def rows_of(k):
        return slice(k * cap, k * cap + cap)

    def y_at(i):
        return lax.rem(y + i, n_y)

    def across_y(i):
        return (me, y_at(i) * 2 + core)

    barrier = pltpu.get_barrier_semaphore()
    peers = [(me, lax.rem(lane + i, n_tp)) for i in range(1, n_tp)]
    peers += [(lax.rem(me + i, n_sp), lane) for i in range(1, n_sp)]
    for other in peers:
        pl.semaphore_signal(barrier, inc=1, device_id=other, device_id_type=MESH)

    def fetch(i):
        src = far[i]
        if i == 13:
            src = src.at[:, cols(lane)]
        return pltpu.make_async_copy(src, near[i], fetched.at[i])

    for i in range(N_IN):
        fetch(i).start()
    for i in range(12):
        fetch(i).wait()

    waits = []

    def go(copy):
        copy.start()
        waits.append(copy)
        return copy

    groups, p_size = damp.shape
    chans = u.shape[0]
    gs = chans // groups
    states = groups * p_size
    tiles = states // 128
    per = 128 // p_size
    n_j = 8
    n_i = tok // n_j

    def lane_group(rows):
        return iota((rows, 128), 1) // p_size

    def as_row(a):
        wide = jnp.concatenate([a] * per, axis=1)
        parts = []
        for tile in range(tiles):
            row = wide[per * tile : per * tile + 1]
            for k in range(1, per):
                row = jnp.where(lane_group(1) == k, wide[per * tile + k : per * tile + k + 1], row)
            parts.append(row)
        return jnp.concatenate(parts, axis=1)

    def spread_tile(columns, tile):
        value = jnp.broadcast_to(columns[:, per * tile : per * tile + 1], (tok, 128))
        for k in range(1, per):
            other = jnp.broadcast_to(columns[:, per * tile + k : per * tile + k + 1], (tok, 128))
            value = jnp.where(lane_group(tok) == k, other, value)
        return value

    block_mask = iota((chans, states), 1) // p_size == iota((chans, states), 0) // gs

    def block_diagonal(a):
        wide = jnp.concatenate([a] * per, axis=1)
        return jnp.where(block_mask, jnp.concatenate([wide] * tiles, axis=1), 0.0)

    eye = where_one(iota((groups, groups), 0) == iota((groups, groups), 1))
    dt = jnp.exp(jnp.sum(eye * log_dt[...], axis=1, keepdims=True))
    a_re, a_im = damp[...], ang[...]
    log_rate = a_re * dt
    angle = a_im * dt
    cos, sin = jnp.cos(angle), jnp.sin(angle)
    half = jnp.sin(0.5 * angle)
    decay = jnp.exp(log_rate)
    num_re = expm1_of(log_rate) * cos - 2.0 * half * half
    num_im = decay * sin
    denom = a_re * a_re + a_im * a_im
    fac_re = as_row((num_re * a_re + num_im * a_im) / denom)
    fac_im = as_row((num_im * a_re - num_re * a_im) / denom)
    lam_re = as_row(decay * cos)
    lam_im = as_row(decay * sin)

    order = iota((tok, tok), 0)
    perm = where_one((order % n_j) * n_i + order // n_j == iota((tok, tok), 1))
    columns = jnp.exp(dot_nt(perm, shrink[...], HIGHEST))
    signal = dot_nt(perm.astype(bf16), u[...])
    in_re, in_im = block_diagonal(ent_re[...]), block_diagonal(ent_im[...])
    drive_re = dot(signal, fac_re * in_re - fac_im * in_im, HIGH)
    drive_im = dot(signal, fac_re * in_im + fac_im * in_re, HIGH)
    row_j = iota((n_j, 128), 0)
    ends = []
    for tile in range(tiles):
        at = slice(128 * tile, 128 * tile + 128)
        modulus = spread_tile(columns, tile)
        t_re, t_im = modulus * lam_re[:, at], modulus * lam_im[:, at]
        for i in range(n_i):
            step = slice(n_j * i, n_j * i + n_j)
            now = (t_re[step], t_im[step], drive_re[step, at], drive_im[step, at])
            run = now if i == 0 else affine_pair(run, now)
            for ref, value in zip((cr, ci, xr, xi), run):
                ref[step, at] = value
        off = 1
        while off < n_j:
            before = [pltpu.roll(value, off, 0) for value in run]
            joined = affine_pair(before, run)
            run = tuple(jnp.where(row_j >= off, new, old) for new, old in zip(joined, run))
            off *= 2
        for plane in range(4):
            mine[plane, tile : tile + 1, :] = run[plane][n_j - 1 : n_j]
        fills = (1.0, 0.0, 0.0, 0.0)
        ends.append(
            [jnp.where(row_j >= 1, pltpu.roll(v, 1, 0), fill) for v, fill in zip(run, fills)]
        )

    pl.semaphore_wait(barrier, len(peers))

    def carry_copy(i):
        return remote(
            mine, pieces.at[i - 1], carry_s.at[i - 1], carry_r.at[i - 1],
            (lax.rem(me + i, n_sp), lane),
        )

    for i in range(1, n_sp):
        @pl.when(me + i < n_sp)
        def _(i=i):
            carry_copy(i).start()

    top = sel.shape[0]
    eye_t = where_one(iota((tok, tok), 0) == iota((tok, tok), 1))
    chosen = dot_nt(eye_t.astype(bf16), sel[...].astype(f32).astype(bf16))
    share = dot_nt(eye_t, scores[...] / jnp.sum(scores[...], axis=0, keepdims=True), HIGHEST)
    index = iota((1, GROUP), 1)
    expert = jnp.where(index < n_sp, xor(me, index, n_sp), -1).astype(f32)
    choice = [chosen[:, k : k + 1] == expert for k in range(top)]
    member = where_one(choice[0])
    part_of = jnp.where(choice[0], share[:, 0:1], 0.0)
    for k in range(1, top):
        member = jnp.where(choice[k], 1.0, member)
        part_of = jnp.where(choice[k], share[:, k : k + 1], part_of)
    below = where_one(iota((tok, tok), 1) <= iota((tok, tok), 0)).astype(bf16)
    rank = (dot(below, member.astype(bf16)) * member).astype(bf16)
    of_slot = where_one(iota((slots, GROUP), 0) // cap == iota((slots, GROUP), 1)).astype(bf16)
    want = (iota((slots, tok), 0) % cap + 1).astype(f32)
    hot[...] = where_one(dot_nt(of_slot, rank) == want).astype(bf16)
    want = (iota((tok, slots), 1) % cap + 1).astype(f32)
    at_slot = dot_nt(part_of.astype(bf16), of_slot)
    weigh[...] = jnp.where(dot_nt(rank, of_slot) == want, at_slot, 0.0).astype(bf16)

    q_re, q_im = block_diagonal(emi_re[...]), block_diagonal(emi_im[...])

    for i in range(1, n_sp):
        @pl.when(me >= i)
        def _(i=i):
            carry_copy(i).wait_recv()
    run_re = jnp.zeros(mine.shape[1:], f32)
    run_im = run_re
    for i in range(n_sp - 1, 0, -1):
        mul_re, mul_im, add_re, add_im = (pieces[i - 1, plane] for plane in range(4))
        new_re = mul_re * run_re - mul_im * run_im + add_re
        new_im = mul_re * run_im + mul_im * run_re + add_im
        run_re = jnp.where(me >= i, new_re, run_re)
        run_im = jnp.where(me >= i, new_im, run_im)

    for tile in range(tiles):
        at = slice(128 * tile, 128 * tile + 128)
        p_re, p_im, z_re, z_im = ends[tile]
        e_re, e_im = run_re[tile : tile + 1], run_im[tile : tile + 1]
        z_re = z_re + p_re * e_re - p_im * e_im
        z_im = z_im + p_re * e_im + p_im * e_re
        for i in range(n_i):
            step = slice(n_j * i, n_j * i + n_j)
            c_re, c_im = cr[step, at], ci[step, at]
            xr[step, at] = xr[step, at] + c_re * z_re - c_im * z_im
            xi[step, at] = xi[step, at] + c_re * z_im + c_im * z_re
    value = dot_nt(xr[...], q_re, HIGH) - dot_nt(xi[...], q_im, HIGH) + signal * bypass[...]
    order = iota((tok, tok), 1)
    back = where_one((order % n_j) * n_i + order // n_j == iota((tok, tok), 0)).astype(bf16)
    mixed_s[...] = dot(back, jax.nn.gelu(value).astype(bf16)).astype(bf16)

    for i in range(12, 15):
        fetch(i).wait()

    def projected_part(block):
        return dot(mixed_s[...], w[:, cols(block)])

    pair = {}
    for i in range(n_y - 1, -1, -1):
        psend_a[i] = projected_part(y_at(i) * 2 + 1 - core).astype(bf16)
        pair[i] = go(remote(psend_a.at[i], precv_a.at[i], pa_s.at[i], pa_r.at[i], partner))
    across = {}
    for i in range(n_y - 1, 0, -1):
        part = projected_part(y_at(i) * 2 + core)
        pair[i].wait_recv()
        ysend_a[i - 1] = (part + precv_a[i].astype(f32)).astype(bf16)
        across[i] = go(
            remote(
                ysend_a.at[i - 1], yrecv_a.at[i - 1], ya_s.at[i - 1], ya_r.at[i - 1], across_y(i)
            )
        )
    total = projected_part(lane)
    pair[0].wait_recv()
    total = total + precv_a[0].astype(f32)
    for i in range(1, n_y):
        across[i].wait_recv()
        total = total + yrecv_a[i - 1].astype(f32)
    stream = (skip[...].astype(f32) + total.astype(bf16).astype(f32)).astype(bf16)
    stream_s[...] = stream
    stream_f = stream.astype(f32)
    square = jnp.sum(stream_f * stream_f, axis=1, keepdims=True)
    as_rows = jnp.broadcast_to(square, (tok, 128)).T[0:8, :]
    ssend[...] = as_rows
    sums = []
    for i in range(1, n_tp):
        sums.append(
            go(
                remote(
                    ssend, srecv.at[i - 1], sum_s.at[i - 1], sum_r.at[i - 1],
                    (me, lax.rem(lane + i, n_tp)),
                )
            )
        )
    scaled = stream_f * gain[0:1, cols(lane)]
    for i, copy in enumerate(sums):
        copy.wait_recv()
        as_rows = as_rows + srecv[i]
    inv = lax.rsqrt(as_rows / width + EPS)
    inv_rms = jnp.broadcast_to(inv[0:1, :], (128, tok)).T[:, 0:1]
    normed = (scaled * inv_rms).astype(bf16)

    def put(k):
        return dot(hot[rows_of(k), :], normed).astype(bf16)

    mine_cols = cols(lane)

    def forward(k):
        here = xs.at[rows_of(k), mine_cols]
        for i in range(1, n_y):
            n = k * (n_y - 1) + i - 1
            go(remote(here, here, f_s.at[n], f_r.at[n], across_y(i)))
        go(remote(here, here, q_s.at[k * n_y], q_r.at[k * n_y], partner))

    xs[rows_of(0), mine_cols] = put(0)
    forward(0)
    for k in range(1, n_sp):
        dsend[k - 1] = put(k)
        go(
            remote(
                dsend.at[k - 1], xs.at[rows_of(k), mine_cols], d_s.at[k - 1], d_r.at[k - 1], peer(k)
            )
        )

    def landed(k, block, send, recv):
        here = xs.at[rows_of(k), cols(block)]
        remote(here, here, send, recv, partner).wait_recv()

    def members(m):
        return range(m * per_group, m * per_group + per_group)

    def step_a(m):
        for k in members(m):
            if k > 0:
                landed(k, lane, d_s.at[k - 1], d_r.at[k - 1])
                forward(k)

    def from_y(i):
        return lax.rem(y + n_y - i, n_y)

    def step_b(m):
        for k in members(m):
            for i in range(1, n_y):
                n = k * (n_y - 1) + i - 1
                block = from_y(i) * 2 + core
                landed(k, block, f_s.at[n], f_r.at[n])
                here = xs.at[rows_of(k), cols(block)]
                go(remote(here, here, q_s.at[k * n_y + i], q_r.at[k * n_y + i], partner))

    pairs, acrosses, backs = {}, {}, {}

    def step_c(m):
        for k in members(m):
            for i in range(n_y):
                block = from_y(i) * 2 + 1 - core
                landed(k, block, q_s.at[k * n_y + i], q_r.at[k * n_y + i])
        rows = xs[m * GROUP : m * GROUP + GROUP, :]
        gate = dot(rows, wg[...])
        hidden = (jax.nn.silu(gate) * dot(rows, wu[...])).astype(bf16)
        order = list(range(1, n_y)) + [0]
        for i in order:
            n = m * n_y + i
            psend[n] = dot(hidden, wd[:, cols(y_at(i) * 2 + 1 - core)]).astype(bf16)
            pairs[n] = go(remote(psend.at[n], precv.at[n], p_s.at[n], p_r.at[n], partner))
        for i in order:
            own[m * n_y + i] = dot(hidden, wd[:, cols(y_at(i) * 2 + core)])

    def step_d(m):
        for i in range(1, n_y):
            n, j = m * n_y + i, m * (n_y - 1) + i - 1
            pairs[n].wait_recv()
            ysend[j] = (own[n] + precv[n].astype(f32)).astype(bf16)
            for k in reversed(members(m)):
                at = pl.ds((k % per_group) * cap, cap)
                s = k * (n_y - 1) + i - 1
                acrosses[k, i] = go(
                    remote(ysend.at[j, at], yrecv.at[j, at], y_s.at[s], y_r.at[s], across_y(i))
                )

    def step_e(m):
        pairs[m * n_y].wait_recv()
        for k in reversed(members(m)):
            at = slice((k % per_group) * cap, (k % per_group) * cap + cap)
            total = own[m * n_y, at] + precv[m * n_y, at].astype(f32)
            for i in range(1, n_y):
                acrosses[k, i].wait_recv()
                total = total + yrecv[m * (n_y - 1) + i - 1, at].astype(f32)
            if k > 0:
                rsend[k - 1] = total.astype(bf16)
                backs[k] = go(
                    remote(
                        rsend.at[k - 1], ret.at[rows_of(k)], r_s.at[k - 1], r_r.at[k - 1], peer(k)
                    )
                )
            else:
                ret[rows_of(0), :] = total.astype(bf16)

    step_a(0)
    step_a(1)
    step_b(0)
    step_b(1)
    step_a(2)
    for i in range(15, 18):
        fetch(i).wait()
    step_c(1)
    step_b(2)
    step_d(1)
    step_a(3)
    step_c(2)
    step_d(2)
    step_b(3)
    step_e(1)
    step_c(3)
    step_d(3)
    step_c(0)
    step_d(0)
    step_e(2)
    step_e(3)
    step_e(0)
    total = stream_s[...].astype(f32)
    for m in list(range(1, n_groups)) + [0]:
        for k in members(m):
            if k > 0:
                backs[k].wait_recv()
        at = slice(m * GROUP, m * GROUP + GROUP)
        total = total + dot(weigh[:, at], ret[at, :])
    out[...] = total.astype(bf16)
    for copy in waits:
        copy.wait_send()
    for i in range(1, n_sp):
        @pl.when(me + i < n_sp)
        def _(i=i):
            carry_copy(i).wait_send()


def layer_call(*args):
    n_sp, n_tp = lax.axis_size("sp"), lax.axis_size("tp")
    n_y = n_tp // 2
    f32, bf16 = jnp.float32, jnp.bfloat16
    tok, width = args[13].shape
    d_local = width // n_tp
    chans = args[0].shape[0]
    groups, p_size = args[1].shape
    states = groups * p_size
    slots = 2 * tok * args[10].shape[0]
    cap = slots // n_sp
    n_groups = slots // GROUP
    more = max(n_y - 1, 1)
    plane = (4, states // 128, 128)
    room = [pltpu.VMEM(a.shape, a.dtype) for a in args]
    room[13] = pltpu.VMEM((tok, d_local), bf16)
    pairs = [n_sp - 1, n_y, more, n_tp - 1, n_sp - 1, n_sp * more, n_sp * n_y, n_groups * n_y]
    pairs += [n_sp * more, n_sp - 1]
    return pl.pallas_call(
        layer_kernel,
        out_shape=jax.ShapeDtypeStruct((tok, d_local), bf16),
        in_specs=[FAR] * N_IN,
        out_specs=VM,
        scratch_shapes=room
        + [DMA((N_IN,))]
        + [pltpu.VMEM((tok, states), f32)] * 4
        + [
            pltpu.VMEM(plane, f32),
            pltpu.VMEM((n_sp - 1,) + plane, f32),
            pltpu.VMEM((tok, chans), bf16),
            pltpu.VMEM((slots, tok), bf16),
            pltpu.VMEM((tok, slots), bf16),
            pltpu.VMEM((tok, d_local), bf16),
            pltpu.VMEM((n_y, tok, d_local), bf16),
            pltpu.VMEM((n_y, tok, d_local), bf16),
            pltpu.VMEM((more, tok, d_local), bf16),
            pltpu.VMEM((more, tok, d_local), bf16),
            pltpu.VMEM((8, tok), f32),
            pltpu.VMEM((n_tp - 1, 8, tok), f32),
            pltpu.VMEM((slots, width), bf16),
            pltpu.VMEM((n_sp - 1, cap, d_local), bf16),
            pltpu.VMEM((n_groups * n_y, GROUP, d_local), bf16),
            pltpu.VMEM((n_groups * n_y, GROUP, d_local), f32),
            pltpu.VMEM((n_groups * n_y, GROUP, d_local), bf16),
            pltpu.VMEM((n_groups * more, GROUP, d_local), bf16),
            pltpu.VMEM((n_groups * more, GROUP, d_local), bf16),
            pltpu.VMEM((n_sp - 1, cap, d_local), bf16),
            pltpu.VMEM((slots, d_local), bf16),
        ]
        + [DMA((n,)) for n in pairs for _ in range(2)],
        compiler_params=pltpu.CompilerParams(
            collective_id=0, has_side_effects=True, vmem_limit_bytes=VMEM_ROOM
        ),
        name="layer",
    )(*args)


def per_device(
    lane_source_signal,
    spectral_damping_part,
    spectral_angular_part,
    interval_exponent,
    entry_matrix_inphase,
    entry_matrix_quadrature,
    emission_inphase,
    emission_quadrature,
    lane_bypass_factor,
    spike_shrink_offset,
    lane_exit_matrix,
    skipline_stream,
    specialist_scaling_vector,
    selected_specialists,
    dispatcher_scores,
    specialist_valve_matrix,
    specialist_widen_matrix,
    specialist_shrink_matrix,
):
    p_size = spectral_damping_part.shape[1]
    return layer_call(
        lane_source_signal,
        spectral_damping_part,
        spectral_angular_part,
        interval_exponent[None, :],
        jnp.swapaxes(entry_matrix_inphase, 1, 2).reshape(-1, p_size),
        jnp.swapaxes(entry_matrix_quadrature, 1, 2).reshape(-1, p_size),
        emission_inphase.reshape(-1, p_size),
        emission_quadrature.reshape(-1, p_size),
        lane_bypass_factor[None, :],
        spike_shrink_offset,
        selected_specialists.T,
        dispatcher_scores.T,
        lane_exit_matrix,
        skipline_stream,
        specialist_scaling_vector[None, :],
        specialist_valve_matrix[0],
        specialist_widen_matrix[0],
        specialist_shrink_matrix[0],
    )


def solution(mesh):
    placed = (
        P("tp", "sp"),
        P("tp", None),
        P("tp", None),
        P("tp"),
        P("tp", None, None),
        P("tp", None, None),
        P("tp", None, None),
        P("tp", None, None),
        P("tp"),
        P("tp", "sp"),
        P("tp", None),
        P("sp", None),
        P(),
        P("sp", None),
        P("sp", None),
        P("sp", None, "tp"),
        P("sp", None, "tp"),
        P("sp", "tp", None),
    )
    return jax.shard_map(
        per_device, mesh=mesh, in_specs=placed, out_specs=P("sp", "tp"), check_vma=False
    )
```

time: 121 us -> 92.4 us (0.76)
  the two profiles are of different devices: /device:TPU:0 before, /device:TPU:9 now
where the time goes in v2:
time: 92.4 us; the launch traced here: 92.3 us
  Pallas kernels  90.6 us (98%)
  local copies, waits for them, and re-layouts  1.67 us (2%)
    pallas_call x1, Pallas kernels, layer_call(): pl.pallas_call(layer_kernel, out_shape=jax.ShapeDtypeStruct((tok, d_local...  90.6 us

profile of v2, /device:TPU:9, one launch (start us, length us, event | category | flops | bytes accessed | tf_op | source)
XLA Modules:
  0.0 92.3 jit_solution(18029192480026693675)
XLA Ops:
  0.0 90.6 %layer.1 = bf16[128,1024]{1,0:T(8,128)(2,1)} custom-call(bf16[256,128]{1,0:T(8,128)(2,1)} %refs_0_.1, f32[16,64]{1,0:T(8,128)} %refs_1_.1, f32[16,64]{1,0:T(8,128)} %refs_2_.1, f32[1,16]{1,0:T(1,128)} %bitcast.27, f32[256,64]{1,0:T(8,128)} %bitcast.19, f32[256,64]{1,0:T(8,128)} %bitcast.20, f32[256,64]{1,0:T(8,128)} %bitcast.21, f32[256,64]{1,0:T(8,128)} %bitcast.22, ...), custom_call_target="tpu_custom_call" | custom-call | tf_op jit(solution)/shard_map/layer/pallas_call | solution.py:488
  90.6 1.7 %copy.20 = bf16[128,1024]{1,0:T(8,128)(2,1)} copy(bf16[128,1024]{1,0:T(8,128)(2,1)} %layer.1) | data formatting | bytes 524288

commit v3 on v2

--- a/solution.py
+++ b/solution.py
@@ -79,8 +79,8 @@
     (
         fetched, xr, xi, cr, ci, mine, pieces, mixed_s, hot, weigh, stream_s,
         psend_a, precv_a, ysend_a, yrecv_a, ssend, srecv,
-        xs, dsend, psend, own, precv, ysend, yrecv, rsend, ret,
-        carry_s, carry_r, pa_s, pa_r, ya_s, ya_r, sum_s, sum_r, d_s, d_r,
+        xs, nsend, nrecv, dsend, psend, own, precv, ysend, yrecv, rsend, ret,
+        carry_s, carry_r, n_s, n_r, pa_s, pa_r, ya_s, ya_r, sum_s, sum_r, d_s, d_r,
         f_s, f_r, q_s, q_r, p_s, p_r, y_s, y_r, r_s, r_r,
     ) = refs[2 * N_IN + 1 :]
     (
@@ -326,16 +326,10 @@
                 )
             )
         )
-    scaled = stream_f * gain[0:1, cols(lane)]
-    for i, copy in enumerate(sums):
-        copy.wait_recv()
-        as_rows = as_rows + srecv[i]
-    inv = lax.rsqrt(as_rows / width + EPS)
-    inv_rms = jnp.broadcast_to(inv[0:1, :], (128, tok)).T[:, 0:1]
-    normed = (scaled * inv_rms).astype(bf16)
+    scaled = (stream_f * gain[0:1, cols(lane)]).astype(bf16)
 
     def put(k):
-        return dot(hot[rows_of(k), :], normed).astype(bf16)
+        return dot(hot[rows_of(k), :], scaled).astype(bf16)
 
     mine_cols = cols(lane)
 
@@ -346,15 +340,40 @@
             go(remote(here, here, f_s.at[n], f_r.at[n], across_y(i)))
         go(remote(here, here, q_s.at[k * n_y], q_r.at[k * n_y], partner))
 
-    xs[rows_of(0), mine_cols] = put(0)
-    forward(0)
-    for k in range(1, n_sp):
+    def dispatch(k):
         dsend[k - 1] = put(k)
         go(
             remote(
                 dsend.at[k - 1], xs.at[rows_of(k), mine_cols], d_s.at[k - 1], d_r.at[k - 1], peer(k)
             )
         )
+
+    first = [n_sp // 2, n_sp // 2 + 1, 1]
+    rest = [k for k in list(range(n_sp // 2, n_sp)) + list(range(1, n_sp // 2)) if k not in first]
+    for k in first[:1]:
+        dispatch(k)
+    xs[rows_of(0), mine_cols] = put(0)
+    forward(0)
+    for k in first[1:]:
+        dispatch(k)
+    for i, copy in enumerate(sums):
+        copy.wait_recv()
+        as_rows = as_rows + srecv[i]
+    inv = lax.rsqrt(as_rows / width + EPS)
+    high = inv.astype(bf16)
+    low = (inv - high.astype(f32)).astype(bf16)
+    by_slot = dot_nt(high, hot[...]) + dot_nt(low, hot[...])
+    part_lane = iota((8, GROUP), 1) // cap
+    for k in range(n_sp):
+        at = slice(k // per_group * GROUP, k // per_group * GROUP + GROUP)
+        scale = jnp.where(part_lane == k % per_group, by_slot[:, at], 0.0)
+        if k == 0:
+            nrecv[0] = scale
+        else:
+            nsend[k - 1] = scale
+            go(remote(nsend.at[k - 1], nrecv.at[k], n_s.at[k - 1], n_r.at[k - 1], peer(k)))
+    for k in rest:
+        dispatch(k)
 
     def landed(k, block, send, recv):
         here = xs.at[rows_of(k), cols(block)]
@@ -388,9 +407,16 @@
             for i in range(n_y):
                 block = from_y(i) * 2 + 1 - core
                 landed(k, block, q_s.at[k * n_y + i], q_r.at[k * n_y + i])
+        for k in members(m):
+            if k > 0:
+                remote(
+                    nrecv.at[k], nrecv.at[k], n_s.at[k - 1], n_r.at[k - 1], partner
+                ).wait_recv()
+            scale = nrecv[k] if k % per_group == 0 else scale + nrecv[k]
+        scale = jnp.broadcast_to(scale[0:1, :], (GROUP, GROUP)).T[:, 0:1]
         rows = xs[m * GROUP : m * GROUP + GROUP, :]
-        gate = dot(rows, wg[...])
-        hidden = (jax.nn.silu(gate) * dot(rows, wu[...])).astype(bf16)
+        gate = dot(rows, wg[...]) * scale
+        hidden = (jax.nn.silu(gate) * (dot(rows, wu[...]) * scale)).astype(bf16)
         order = list(range(1, n_y)) + [0]
         for i in order:
             n = m * n_y + i
@@ -430,35 +456,35 @@
                 ret[rows_of(0), :] = total.astype(bf16)
 
     step_a(0)
+    step_a(2)
+    step_b(0)
     step_a(1)
-    step_b(0)
-    step_b(1)
-    step_a(2)
+    step_b(2)
     for i in range(15, 18):
         fetch(i).wait()
-    step_c(1)
-    step_b(2)
-    step_d(1)
-    step_a(3)
     step_c(2)
     step_d(2)
+    step_b(1)
+    step_c(1)
+    step_a(3)
+    step_e(2)
+    step_d(1)
     step_b(3)
+    step_c(3)
     step_e(1)
-    step_c(3)
     step_d(3)
     step_c(0)
     step_d(0)
-    step_e(2)
     step_e(3)
     step_e(0)
     total = stream_s[...].astype(f32)
-    for m in list(range(1, n_groups)) + [0]:
+    for m in [2, 1, 3, 0]:
         for k in members(m):
             if k > 0:
                 backs[k].wait_recv()
         at = slice(m * GROUP, m * GROUP + GROUP)
         total = total + dot(weigh[:, at], ret[at, :])
-    out[...] = total.astype(bf16)
+    out[...] = total
     for copy in waits:
         copy.wait_send()
     for i in range(1, n_sp):
@@ -483,11 +509,11 @@
     plane = (4, states // 128, 128)
     room = [pltpu.VMEM(a.shape, a.dtype) for a in args]
     room[13] = pltpu.VMEM((tok, d_local), bf16)
-    pairs = [n_sp - 1, n_y, more, n_tp - 1, n_sp - 1, n_sp * more, n_sp * n_y, n_groups * n_y]
+    pairs = [n_sp - 1, n_sp - 1, n_y, more, n_tp - 1, n_sp - 1, n_sp * more, n_sp * n_y, n_groups * n_y]
     pairs += [n_sp * more, n_sp - 1]
     return pl.pallas_call(
         layer_kernel,
-        out_shape=jax.ShapeDtypeStruct((tok, d_local), bf16),
+        out_shape=jax.ShapeDtypeStruct((tok, d_local), f32),
         in_specs=[FAR] * N_IN,
         out_specs=VM,
         scratch_shapes=room
@@ -507,6 +533,8 @@
             pltpu.VMEM((8, tok), f32),
             pltpu.VMEM((n_tp - 1, 8, tok), f32),
             pltpu.VMEM((slots, width), bf16),
+            pltpu.VMEM((n_sp - 1, 8, GROUP), f32),
+            pltpu.VMEM((n_sp, 8, GROUP), f32),
             pltpu.VMEM((n_sp - 1, cap, d_local), bf16),
             pltpu.VMEM((n_groups * n_y, GROUP, d_local), bf16),
             pltpu.VMEM((n_groups * n_y, GROUP, d_local), f32),
@@ -545,7 +573,7 @@
     specialist_shrink_matrix,
 ):
     p_size = spectral_damping_part.shape[1]
-    return layer_call(
+    total = layer_call(
         lane_source_signal,
         spectral_damping_part,
         spectral_angular_part,
@@ -565,6 +593,7 @@
         specialist_widen_matrix[0],
         specialist_shrink_matrix[0],
     )
+    return total.astype(jnp.bfloat16)
 
 
 def solution(mesh):

time: 92.4 us -> 87.3 us (0.945)
  the two profiles are of different devices: /device:TPU:9 before, /device:TPU:0 now
where the time goes in v3:
time: 87.3 us; the launch traced here: 87.2 us
  Pallas kernels  85.4 us (98%)
  other arithmetic  1.78 us (2%)
    pallas_call x1, Pallas kernels, layer_call(): pl.pallas_call(layer_kernel, out_shape=jax.ShapeDtypeStruct((tok, d_local...  85.4 us
    convert_element_type x1, other arithmetic, per_device(): return total.astype(jnp.bfloat16)  1.78 us

profile of v3, /device:TPU:0, one launch (start us, length us, event | category | flops | bytes accessed | tf_op | source)
XLA Modules:
  0.0 87.2 jit_solution(2721611508171288143)
XLA Ops:
  0.0 85.4 %layer.1 = f32[128,1024]{1,0:T(8,128)} custom-call(bf16[256,128]{1,0:T(8,128)(2,1)} %refs_0_.1, f32[16,64]{1,0:T(8,128)} %refs_1_.1, f32[16,64]{1,0:T(8,128)} %refs_2_.1, f32[1,16]{1,0:T(1,128)} %bitcast.27, f32[256,64]{1,0:T(8,128)} %bitcast.19, f32[256,64]{1,0:T(8,128)} %bitcast.20, f32[256,64]{1,0:T(8,128)} %bitcast.21, f32[256,64]{1,0:T(8,128)} %bitcast.22, ...), custom_call_target="tpu_custom_call" | custom-call | tf_op jit(solution)/shard_map/layer/pallas_call | solution.py:514
  85.4 1.8 %convert_element_type.3 = bf16[128,1024]{1,0:T(8,128)(2,1)} convert(f32[128,1024]{1,0:T(8,128)} %layer.1) | non-fusion elementwise | flops 131072 | bytes 786432 | tf_op jit(solution)/shard_map/convert_element_type | solution.py:596

commit v4 on v3

--- a/solution.py
+++ b/solution.py
@@ -10,7 +10,7 @@
 VM = pl.BlockSpec(memory_space=pltpu.VMEM)
 FAR = pl.BlockSpec(memory_space=pl.ANY)
 DMA = pltpu.SemaphoreType.DMA
-VMEM_ROOM = 60 * 1024 * 1024
+VMEM_ROOM = 48 * 1024 * 1024
 HIGH, HIGHEST = lax.Precision.HIGH, lax.Precision.HIGHEST
 GROUP = 128
 
@@ -349,7 +349,7 @@
         )
 
     first = [n_sp // 2, n_sp // 2 + 1, 1]
-    rest = [k for k in list(range(n_sp // 2, n_sp)) + list(range(1, n_sp // 2)) if k not in first]
+    rest = [k for k in list(range(2, n_sp)) if k not in first]
     for k in first[:1]:
         dispatch(k)
     xs[rows_of(0), mine_cols] = put(0)
@@ -459,9 +459,10 @@
     step_a(2)
     step_b(0)
     step_a(1)
-    step_b(2)
     for i in range(15, 18):
         fetch(i).wait()
+    step_c(0)
+    step_b(2)
     step_c(2)
     step_d(2)
     step_b(1)
@@ -473,7 +474,6 @@
     step_c(3)
     step_e(1)
     step_d(3)
-    step_c(0)
     step_d(0)
     step_e(3)
     step_e(0)
@@ -549,7 +549,7 @@
             collective_id=0, has_side_effects=True, vmem_limit_bytes=VMEM_ROOM
         ),
         name="layer",
-    )(*args)
+    )(*[pltpu.with_memory_space_constraint(a, pltpu.HBM) for a in args])
 
 
 def per_device(

time: 87.3 us -> 83.8 us (0.960)
  Pallas kernels: 85.4 us -> 82.9 us
  other arithmetic: 1.78 us -> 0.74 us
    pallas_call x1, Pallas kernels: 85.4 us -> 82.9 us  [layer_call(): pl.pallas_call(layer_kernel, out_shape=jax.ShapeDtypeStruct((tok, d_local...]
    convert_element_type x1, other arithmetic: 1.78 us -> 0.74 us  [per_device(): return total.astype(jnp.bfloat16)]
where the time goes in v4:
time: 83.8 us; the launch traced here: 83.7 us
  Pallas kernels  82.9 us (99%)
    pallas_call x1, Pallas kernels, layer_call(): pl.pallas_call(layer_kernel, out_shape=jax.ShapeDtypeStruct((tok, d_local...  82.9 us

profile of v4, /device:TPU:0, one launch (start us, length us, event | category | flops | bytes accessed | tf_op | source)
XLA Modules:
  0.0 83.7 jit_solution(17320112040683532933)
XLA Ops:
  0.0 82.9 %layer.1 = f32[128,1024]{1,0:T(8,128)S(1)} custom-call(bf16[256,128]{1,0:T(8,128)(2,1)} %refs_0_.1, f32[16,64]{1,0:T(8,128)} %refs_1_.1, f32[16,64]{1,0:T(8,128)} %refs_2_.1, f32[1,16]{1,0:T(1,128)} %bitcast.27, f32[256,64]{1,0:T(8,128)} %bitcast.19, f32[256,64]{1,0:T(8,128)} %bitcast.20, f32[256,64]{1,0:T(8,128)} %bitcast.21, f32[256,64]{1,0:T(8,128)} %bitcast.22, ...), custom_call_target="tpu_custom_call" | custom-call | tf_op jit(solution)/shard_map/layer/pallas_call | solution.py:514
  83.0 0.7 convert_element_type.3

commit v5 on v4

--- a/solution.py
+++ b/solution.py
@@ -348,7 +348,7 @@
             )
         )
 
-    first = [n_sp // 2, n_sp // 2 + 1, 1]
+    first = list(dict.fromkeys([n_sp // 2, 2, n_sp // 2 + 1, 1]))
     rest = [k for k in list(range(2, n_sp)) if k not in first]
     for k in first[:1]:
         dispatch(k)

time: 83.8 us -> 80.8 us (0.964)
  Pallas kernels: 82.9 us -> 79.9 us
    pallas_call x1, Pallas kernels: 82.9 us -> 79.9 us  [layer_call(): pl.pallas_call(layer_kernel, out_shape=jax.ShapeDtypeStruct((tok, d_local...]
where the time goes in v5:
time: 80.8 us; the launch traced here: 80.6 us
  Pallas kernels  79.9 us (99%)
    pallas_call x1, Pallas kernels, layer_call(): pl.pallas_call(layer_kernel, out_shape=jax.ShapeDtypeStruct((tok, d_local...  79.9 us

profile of v5, /device:TPU:0, one launch (start us, length us, event | category | flops | bytes accessed | tf_op | source)
XLA Modules:
  0.0 80.6 jit_solution(8942210274291198505)
XLA Ops:
  0.0 79.9 %layer.1 = f32[128,1024]{1,0:T(8,128)S(1)} custom-call(bf16[256,128]{1,0:T(8,128)(2,1)} %refs_0_.1, f32[16,64]{1,0:T(8,128)} %refs_1_.1, f32[16,64]{1,0:T(8,128)} %refs_2_.1, f32[1,16]{1,0:T(1,128)} %bitcast.27, f32[256,64]{1,0:T(8,128)} %bitcast.19, f32[256,64]{1,0:T(8,128)} %bitcast.20, f32[256,64]{1,0:T(8,128)} %bitcast.21, f32[256,64]{1,0:T(8,128)} %bitcast.22, ...), custom_call_target="tpu_custom_call" | custom-call | tf_op jit(solution)/shard_map/layer/pallas_call | solution.py:514
  79.9 0.7 convert_element_type.3
